TPU v7x, 512 devices: a whole 4x4x16 slice. The times are simulated.
512 devices in a mesh: ep: 128 (over z, x, core), tp: 4 (over y).
Axes of the slice: x: 4, y: 4, z: 16, core: 2. Of those that a mesh axis runs over, the one named last changes fastest.
Arguments:
- tokens: bfloat16 [16384, 1024], P('ep', 'tp'), may hold values from -6 to 6
- cotangent: bfloat16 [16384, 1024], P('ep', 'tp'), may hold values from -12 to 12
- routes: int32 [16384, 2], P('ep'), may hold values from 0 to 63, all different within a row; in each aligned block of 128 rows (0 to 127, 128 to 255, ...) at most 5 rows name the same one
- route_weights: bfloat16 [16384, 2], P('ep'), may hold values from 0.099609375 to 0.8984375
- w_gate: bfloat16 [128, 1024, 1408], P('ep', None, 'tp'), may hold values from -0.1875 to 0.1875
- w_up: bfloat16 [128, 1024, 1408], P('ep', None, 'tp'), may hold values from -0.1875 to 0.1875
- w_down: bfloat16 [128, 1408, 1024], P('ep', 'tp'), may hold values from -0.109375 to 0.109375
- dense_weight: bfloat16 [1024, 1024], P('tp', 'ep'), may hold values from -0.75 to 0.75
- mix_gate: float32 [1024], replicated, may hold values from 0.1 to 1.9
Outputs:
- token_grad: bfloat16 [16384, 1024], P('ep', 'tp')
- route_grad: float32 [16384, 2], P('ep')
- gate_grad: bfloat16 [128, 1024, 1408], P('ep', None, 'tp')
- up_grad: bfloat16 [128, 1024, 1408], P('ep', None, 'tp')
- down_grad: bfloat16 [128, 1408, 1024], P('ep', 'tp')
- dense_grad: float32 [1024, 1024], P('tp', 'ep')
- mix_grad: float32 [1024], replicated
Inputs may be any that keep to these rules, and one draw needn't show every extreme that they name: `routes`: each row names 2 different experts. In the rows of one index of ep (aligned blocks of 128 rows) no expert is named by more than 5 rows, a bound that some block reaches.
All inputs are finite; a program needn't handle non-finite values.
Results may differ from a plain program's by a relative error of at most 0.0065.
Values may be sent and summed in bfloat16 or wider, within the bound.
A program may use at most 64 MiB of HBM per device.

v0:
```python
import functools

import jax
import jax.numpy as jnp
from jax import lax
from jax.sharding import Mesh
from jax.sharding import PartitionSpec as P

FF = 2816
EP = ("ep_0", "ep_1", "ep_2")
EP_TP = ("ep_0", "ep_1", "ep_2", "tp")


def split_up(value, dim, peers):
    before, after = (value.shape[:dim], value.shape[dim + 1 :])
    return jnp.moveaxis(value.reshape(*before, peers, -1, *after), dim, 0)


def joined_along(pieces, dim):
    lengths = list(pieces.shape[1:])
    lengths[dim] *= pieces.shape[0]
    return jnp.moveaxis(pieces, 0, dim).reshape(lengths)


def exchange_in_order(pieces, axes, order):
    lengths = [lax.axis_size(a) for a in axes]
    pieces = pieces.reshape(*lengths, *pieces.shape[1:])
    for k in order:
        pieces = lax.all_to_all(pieces, axes[k], split_axis=k, concat_axis=k, tiled=True)
    return pieces.reshape(-1, *pieces.shape[len(axes) :])


def two_step_exchange(value, groups, order, split_dim, concat_dim):
    peers = lax.axis_size(groups[0]) * lax.axis_size(groups[1])
    pieces = split_up(value, split_dim, peers)
    return joined_along(exchange_in_order(pieces, groups, order), concat_dim)


def stacked_from(value, axes, order):
    pieces = value
    for k in order:
        pieces = lax.all_gather(pieces, axes[k])
    done = order[::-1]
    back = [done.index(k) for k in range(len(axes))]
    pieces = pieces.transpose(*back, *range(len(axes), pieces.ndim))
    return pieces.reshape(-1, *value.shape)


def whole_of(value, axes, order, dim):
    return joined_along(stacked_from(value, axes, order), dim)


def over_axes(value, axes):
    return functools.reduce(lax.psum, axes, value)


def own_tiles(value, axis, dim):
    peers = lax.axis_size(axis)
    pieces = split_up(value, dim, peers)
    length = value.size // peers
    spare = max(2048 - length, -length % 1024)
    padded = jnp.pad(pieces.reshape(peers, length), ((0, 0), (0, spare)))
    own = lax.psum_scatter(padded.reshape(-1, 128), axis, scatter_dimension=0, tiled=True)
    return own.reshape(-1)[:length].reshape(pieces.shape[1:])


def spread(values, experts, group_size):
    capacity = values.shape[0] // experts
    shaped = values.reshape((experts, 1, capacity) + values.shape[1:])
    copies = jnp.broadcast_to(shaped, (experts, group_size, capacity) + values.shape[1:])
    return copies.reshape((experts * group_size * capacity,) + values.shape[1:])


def local(tokens, cotangent, routes, route_weights, w_gate, w_up, w_down, dense_weight, mix_gate):
    tp_count = lax.axis_size("tp")
    ep_count = lax.axis_size(EP)
    slice_width = w_gate.shape[2]
    group_size = FF // (slice_width * tp_count)
    experts = ep_count // group_size
    token_count, top_count = routes.shape
    capacity = 5 * token_count * top_count // (4 * experts)
    picked = routes.reshape(-1)
    onehot = (picked[:, None] == jnp.arange(experts, dtype=jnp.int32)[None, :]).astype(jnp.int32)
    ranking = jnp.cumsum(onehot, axis=0) - 1
    target = picked * capacity + jnp.sum(onehot * ranking, axis=1)
    matches = (target[:, None] == jnp.arange(experts * capacity, dtype=jnp.int32)[None, :]).astype(
        jnp.int32
    )
    pick_index = jnp.arange(picked.shape[0], dtype=jnp.int32)
    pick_of = jnp.sum(matches * pick_index[:, None], axis=0)
    filled = jnp.sum(matches, axis=0)
    token_of = pick_of // top_count
    slot_weight = jnp.take(route_weights.reshape(-1), pick_of, axis=0) * filled.astype(jnp.bfloat16)
    weight_out = spread(slot_weight, experts, group_size)
    grads_full = lax.all_gather(cotangent, "tp", axis=1, tiled=True)
    rows_part, grads_in, weights_in = (
        lax.all_to_all(
            spread(jnp.take(tokens, token_of, axis=0), experts, group_size),
            EP,
            split_axis=0,
            concat_axis=0,
            tiled=True,
        ),
        lax.all_to_all(
            spread(jnp.take(grads_full, token_of, axis=0), experts, group_size),
            EP,
            split_axis=0,
            concat_axis=0,
            tiled=True,
        ),
        lax.all_to_all(weight_out, EP, split_axis=0, concat_axis=0, tiled=True),
    )
    rows_in = lax.all_gather(rows_part, "tp", axis=1, tiled=True)
    gate_matrix = w_gate[0]
    up_matrix = w_up[0]
    down_matrix = w_down[0]
    pre_gate = jnp.dot(rows_in, gate_matrix, preferred_element_type=jnp.float32)
    pre_up = jnp.dot(rows_in, up_matrix, preferred_element_type=jnp.float32)
    sigmoid_gate = jax.nn.sigmoid(pre_gate)
    activated = pre_gate * sigmoid_gate
    hidden = activated * pre_up
    hidden_bf = hidden.astype(jnp.bfloat16)
    projected = lax.dot_general(
        grads_in, down_matrix, (((1,), (1,)), ((), ())), preferred_element_type=jnp.float32
    )
    route_part = jnp.sum(hidden_bf.astype(jnp.float32) * projected, axis=1)
    weight_col = weights_in.astype(jnp.float32)[:, None]
    hidden_grad = weight_col * projected
    d_gate = (hidden_grad * pre_up * sigmoid_gate * (1.0 + pre_gate * (1.0 - sigmoid_gate))).astype(
        jnp.bfloat16
    )
    d_up = (hidden_grad * activated).astype(jnp.bfloat16)
    weighted = (weight_col * hidden).astype(jnp.bfloat16)
    contract_rows = (((0,), (0,)), ((), ()))
    gate_grad = lax.dot_general(
        rows_in, d_gate, contract_rows, preferred_element_type=jnp.float32
    ).astype(jnp.bfloat16)[None]
    up_grad = lax.dot_general(
        rows_in, d_up, contract_rows, preferred_element_type=jnp.float32
    ).astype(jnp.bfloat16)[None]
    down_grad = lax.dot_general(
        weighted, grads_in, contract_rows, preferred_element_type=jnp.float32
    ).astype(jnp.bfloat16)[None]
    contract_cols = (((1,), (1,)), ((), ()))
    partial_value = (
        lax.dot_general(d_gate, gate_matrix, contract_cols, preferred_element_type=jnp.float32)
        + lax.dot_general(d_up, up_matrix, contract_cols, preferred_element_type=jnp.float32)
    ).astype(jnp.bfloat16)
    mixed = lax.all_to_all(partial_value, "tp", split_axis=1, concat_axis=0, tiled=True)
    rows_here = partial_value.shape[0]
    column_sum = jnp.sum(mixed.reshape(tp_count, rows_here, -1).astype(jnp.float32), axis=0).astype(
        jnp.bfloat16
    )
    route_sum = lax.psum(route_part, "tp")
    returned = lax.all_to_all(column_sum, EP, split_axis=0, concat_axis=0, tiled=True)
    route_back = two_step_exchange(route_sum, (("ep_0", "ep_1"), "ep_2"), (1, 0), 0, 0)
    slot_grad = jnp.sum(
        returned.reshape(experts, group_size, capacity, -1).astype(jnp.float32), axis=1
    ).reshape(experts * capacity, -1)
    slot_route = jnp.sum(route_back.reshape(experts, group_size, capacity), axis=1).reshape(-1)
    expert_grad = jnp.sum(
        jnp.take(slot_grad, target, axis=0).reshape(token_count, top_count, -1), axis=1
    )
    route_grad = jnp.take(slot_route, target, axis=0).reshape(token_count, top_count)
    scaled = (mix_gate[None, :] * grads_full.astype(jnp.float32)).astype(jnp.bfloat16)
    moment = lax.dot_general(tokens, grads_full, contract_rows, preferred_element_type=jnp.float32)
    shard_piece = whole_of(dense_weight, EP, (1, 0, 2), 1)
    scaled_cols = scaled
    dense_acc = lax.dot_general(
        scaled_cols, shard_piece, contract_cols, preferred_element_type=jnp.float32
    )
    gain_cols = jnp.sum(shard_piece.astype(jnp.float32) * moment, axis=0)
    gain_part = gain_cols
    dense_dx, gain_part = (dense_acc, gain_part)
    mix_grad = over_axes(gain_part, EP_TP) / ep_count
    scaled_cols = scaled
    product = lax.dot_general(
        scaled_cols, tokens, contract_rows, preferred_element_type=jnp.float32
    )
    dense_rows_sum = own_tiles(product * (1.0 / ep_count), EP, 0)
    dense_grad = dense_rows_sum.T
    token_grad = (expert_grad + dense_dx).astype(jnp.bfloat16)
    return (token_grad, route_grad, gate_grad, up_grad, down_grad, dense_grad, mix_grad)


def solution(mesh):
    finer = Mesh(mesh.devices.reshape(16, 4, 2, mesh.shape["tp"]), ("ep_0", "ep_1", "ep_2", "tp"))
    in_specs = (
        P(EP, "tp"),
        P(EP, "tp"),
        P(EP, None),
        P(EP, None),
        P(EP, None, "tp"),
        P(EP, None, "tp"),
        P(EP, "tp", None),
        P("tp", EP),
        P(),
    )
    out_specs = (
        P(EP, "tp"),
        P(EP, None),
        P(EP, None, "tp"),
        P(EP, None, "tp"),
        P(EP, "tp", None),
        P("tp", EP),
        P(),
    )
    return jax.shard_map(local, mesh=finer, in_specs=in_specs, out_specs=out_specs, check_vma=False)
```

profile of v0, /device:TPU:1, one launch (start us, length us, event | category | flops | bytes accessed | tf_op | source)
XLA Modules:
  0.0 394.9 jit_solution(6875033105968997943)
XLA Ops:
  8.0 0.9 copy.67
  11.5 2.4 gather_fusion
  14.9 20.4 %all-to-all-start = ((bf16[128,5,1]{1,2,0:T(2,128)(2,1)}), bf16[128,5,1]{1,2,0:T(2,128)(2,1)S(1)}, u32[]{:S(2)}, u32[]{:S(2)}) async-start(bf16[128,5,1]{1,2,0:T(2,128)(2,1)} %copy.72), calls=%async_computation | async-start | bytes 131072 | tf_op jit(solution)/shard_map/all_to_all | solution.py:111
  35.4 2.0 gather_fusion.2
  37.6 12.5 %all-to-all-done = bf16[128,5,1]{1,2,0:T(2,128)(2,1)S(1)} async-done(((bf16[128,5,1]{1,2,0:T(2,128)(2,1)}), bf16[128,5,1]{1,2,0:T(2,128)(2,1)S(1)}, u32[]{:S(2)}, u32[]{:S(2)}) %all-to-all-start) | async-done | bytes 1312 | tf_op jit(solution)/shard_map/all_to_all | solution.py:111
  50.1 0.8 broadcast_in_dim.80
  51.0 6.8 %all-to-all-start.2 = ((bf16[128,5,256]{2,1,0:T(8,128)(2,1)}), bf16[128,5,256]{2,1,0:T(8,128)(2,1)}, u32[]{:S(2)}, u32[]{:S(2)}) async-start(bf16[128,5,256]{2,1,0:T(8,128)(2,1)} %bitcast.4), calls=%async_computation.2 | async-start | bytes 1048576 | tf_op jit(solution)/shard_map/all_to_all | solution.py:97
  57.8 11.3 %all_gather.24 = bf16[128,1024]{1,0:T(8,128)(2,1)S(1)} all-gather(bf16[128,256]{1,0:T(8,128)(2,1)S(1)} %copy-done.8), channel_id=1, replica_groups=mesh['ep_0'=16,'ep_1'=4,'ep_2'=2,'tp'=4] {'tp'}, dimensions={1}, use_global_device_ids=true | all-gather | bytes 327680 | tf_op jit(solution)/shard_map/all_gather | solution.py:95
  69.1 2.1 gather_fusion.1
  71.6 16.9 %all-to-all-done.2 = bf16[128,5,256]{2,1,0:T(8,128)(2,1)} async-done(((bf16[128,5,256]{2,1,0:T(8,128)(2,1)}), bf16[128,5,256]{2,1,0:T(8,128)(2,1)}, u32[]{:S(2)}, u32[]{:S(2)}) %all-to-all-start.2) | async-done | bytes 327712 | tf_op jit(solution)/shard_map/all_to_all | solution.py:97
  88.6 1.6 broadcast_in_dim.77
  90.2 9.1 %all-to-all-start.1 = ((bf16[128,5,1024]{2,1,0:T(8,128)(2,1)}), bf16[128,5,1024]{2,1,0:T(8,128)(2,1)S(1)}, u32[]{:S(2)}, u32[]{:S(2)}) async-start(bf16[128,5,1024]{2,1,0:T(8,128)(2,1)} %bitcast.75), calls=%async_computation.1 | async-start | bytes 4194304 | tf_op jit(solution)/shard_map/all_to_all | solution.py:104
  99.3 1.9 all_to_all.51
  101.3 1.3 convolution_multiply_fusion.1
  102.7 2.3 reshape.275
  105.0 10.0 %all-gather = bf16[1024,8]{0,1:T(8,128)(2,1)S(1)} all-gather(bf16[256,8]{0,1:T(8,128)(2,1)S(1)} %copy-done.10), channel_id=2, replica_groups=mesh['ep_0'=16,'ep_1'=4,'ep_2'=2,'tp'=4] {'ep_1'}, dimensions={0}, use_global_device_ids=true | all-gather | bytes 20480 | tf_op jit(solution)/shard_map/all_gather | solution.py:42
  115.1 95.5 %all-gather.1 = bf16[64,256,8]{1,2,0:T(8,128)(2,1)S(1)} all-gather(bf16[4,256,8]{1,2,0:T(8,128)(2,1)S(1)} %bitcast.83), channel_id=3, replica_groups=mesh['ep_0'=16,'ep_1'=4,'ep_2'=2,'tp'=4] {'ep_0'}, dimensions={0}, use_global_device_ids=true | all-gather | bytes 278528 | tf_op jit(solution)/shard_map/all_gather | solution.py:42
  210.5 7.8 %all-gather.2 = bf16[32,4,256,8]{2,3,1,0:T(8,128)(2,1)S(1)} all-gather(bf16[16,4,256,8]{2,3,1,0:T(8,128)(2,1)S(1)} %bitcast.81), channel_id=4, replica_groups=mesh['ep_0'=16,'ep_1'=4,'ep_2'=2,'tp'=4] {'ep_2'}, dimensions={0}, use_global_device_ids=true | all-gather | bytes 786432 | tf_op jit(solution)/shard_map/all_gather | solution.py:42
  218.4 0.8 copy.74
  219.2 2.0 copy.79
  221.2 1.4 fusion.3
  222.6 21.4 %psum.36 = f32[1024]{0:T(1024)S(1)} all-reduce(f32[1024]{0:T(1024)S(1)} %fusion.3), channel_id=1, replica_groups=mesh['ep_0'=16,'ep_1'=4,'ep_2'=2,'tp'=4] {'ep_0'}, use_global_device_ids=true, to_apply=%region_13.14 | all-reduce | flops 1024 | bytes 8192 | tf_op jit(solution)/shard_map/psum | solution.py:54
  244.0 8.9 %psum.37 = f32[1024]{0:T(1024)S(1)} all-reduce(f32[1024]{0:T(1024)S(1)} %psum.36), channel_id=1, replica_groups=mesh['ep_0'=16,'ep_1'=4,'ep_2'=2,'tp'=4] {'ep_1'}, use_global_device_ids=true, to_apply=%region_14.15 | all-reduce | flops 1024 | bytes 8192 | tf_op jit(solution)/shard_map/psum | solution.py:54
  252.9 11.8 %psum.38 = f32[1024]{0:T(1024)S(1)} all-reduce(f32[1024]{0:T(1024)S(1)} %psum.37), channel_id=1, replica_groups=mesh['ep_0'=16,'ep_1'=4,'ep_2'=2,'tp'=4] {'ep_2'}, use_global_device_ids=true, to_apply=%region_15.16 | all-reduce | flops 1024 | bytes 8192 | tf_op jit(solution)/shard_map/psum | solution.py:54
  265.1 3.2 fusion.8
  268.3 1.7 fusion.11
  270.0 1.4 all_to_all.48
  271.4 3.1 multiply_reduce_fusion
  274.8 14.6 %all-reduce = (f32[64,2,5]{2,1,0:T(2,128)S(1)}, f32[1024]{0:T(1024)S(1)}) all-reduce(f32[64,2,5]{2,1,0:T(2,128)S(1)} %reshape_reshape.7, f32[1024]{0:T(1024)S(1)} %psum.38), channel_id=1, replica_groups=mesh['ep_0'=16,'ep_1'=4,'ep_2'=2,'tp'=4] {'tp'}, use_global_device_ids=true, to_apply=%region_9.10 | all-reduce | flops 1664 | bytes 13312 | tf_op jit(solution)/shard_map/psum | solution.py:154
  290.1 7.0 %all-to-all-start.5 = ((f32[2,1,320]{2,1,0:T(1,128)}), f32[2,1,320]{2,1,0:T(1,128)S(1)}, u32[]{:S(2)}, u32[]{:S(2)}) async-start(f32[2,1,320]{2,1,0:T(1,128)} %reshape.331), calls=%async_computation.5 | async-start | bytes 6144 | tf_op jit(solution)/shard_map/all_to_all | solution.py:29
  297.1 0.9 fusion.6
  298.2 0.9 add_convert_fusion
  299.1 1.1 copy.86
  300.3 3.5 all-to-all-start.3
  306.0 15.8 %all-to-all-done.3 = bf16[640,4,256]{2,0,1:T(8,128)(2,1)S(1)} async-done(((bf16[640,4,256]{2,0,1:T(8,128)(2,1)}), bf16[640,4,256]{2,0,1:T(8,128)(2,1)S(1)}, u32[]{:S(2)}, u32[]{:S(2)}) %all-to-all-start.3) | async-done | bytes 1310752 | tf_op jit(solution)/shard_map/all_to_all | solution.py:149
  321.8 10.1 %all-to-all-start.6 = ((f32[64,2,5]{2,1,0:T(2,128)}), f32[64,2,5]{2,1,0:T(2,128)S(1)}, u32[]{:S(2)}, u32[]{:S(2)}) async-start(f32[64,2,5]{2,1,0:T(2,128)} %copy.76), calls=%async_computation.6 | async-start | bytes 131072 | tf_op jit(solution)/shard_map/all_to_all | solution.py:29
  332.2 1.0 all_to_all.54
  333.2 13.0 %all-to-all-done.6 = f32[64,2,5]{2,1,0:T(2,128)S(1)} async-done(((f32[64,2,5]{2,1,0:T(2,128)}), f32[64,2,5]{2,1,0:T(2,128)S(1)}, u32[]{:S(2)}, u32[]{:S(2)}) %all-to-all-start.6) | async-done | bytes 2592 | tf_op jit(solution)/shard_map/all_to_all | solution.py:29
  346.2 7.2 %all-to-all-start.4 = ((bf16[128,5,256]{2,1,0:T(8,128)(2,1)}), bf16[128,5,256]{2,1,0:T(8,128)(2,1)S(1)}, u32[]{:S(2)}, u32[]{:S(2)}) async-start(bf16[128,5,256]{2,1,0:T(8,128)(2,1)} %all_to_all.54), calls=%async_computation.4 | async-start | bytes 1048576 | tf_op jit(solution)/shard_map/all_to_all | solution.py:155
  353.6 7.5 %reduce-scatter.2.cloned.1.call-done = f32[16,128]{1,0:T(8,128)} async-done(((f32[2048,128]{1,0:T(8,128)}), f32[16,128]{1,0:T(8,128)}) %reduce-scatter.2.cloned.1.call-update) | async-done | bytes 8208 | tf_op jit(solution)/shard_map/reduce_scatter | solution.py:63
  361.0 1.3 reshape_reshape.8
  362.9 3.1 fusion.1
  366.0 1.6 fusion.2
  367.6 1.7 fusion
  369.5 1.9 gather_fusion.4
  372.2 12.6 %all-to-all-done.4 = bf16[128,5,256]{2,1,0:T(8,128)(2,1)S(1)} async-done(((bf16[128,5,256]{2,1,0:T(8,128)(2,1)}), bf16[128,5,256]{2,1,0:T(8,128)(2,1)S(1)}, u32[]{:S(2)}, u32[]{:S(2)}) %all-to-all-start.4) | async-done | bytes 327712 | tf_op jit(solution)/shard_map/all_to_all | solution.py:155
  385.0 1.0 gather_fusion.3
  386.6 0.9 fusion.4
  (89 shorter events, 11.1 us)
Async XLA Ops:
  8.0 257.1 %copy-start = (bf16[1,1024,352]{1,2,0:T(8,128)(2,1)S(1)}, bf16[1,1024,352]{1,2,0:T(8,128)(2,1)}, u32[]{:S(2)}) copy-start(bf16[1,1024,352]{1,2,0:T(8,128)(2,1)} %param.13) | copy-start | bytes 2162692
  8.0 27.3 %copy-start.1 = (bf16[128,256]{1,0:T(8,128)(2,1)S(1)}, bf16[128,256]{1,0:T(8,128)(2,1)}, u32[]{:S(2)}) copy-start(bf16[128,256]{1,0:T(8,128)(2,1)} %param.9) | copy-start | bytes 196612
  14.9 35.2 %all-to-all-start = ((bf16[128,5,1]{1,2,0:T(2,128)(2,1)}), bf16[128,5,1]{1,2,0:T(2,128)(2,1)S(1)}, u32[]{:S(2)}, u32[]{:S(2)}) async-start(bf16[128,5,1]{1,2,0:T(2,128)(2,1)} %copy.72), calls=%async_computation | async-start | bytes 131072 | tf_op jit(solution)/shard_map/all_to_all | solution.py:111
  37.4 20.4 %copy-start.8 = (bf16[128,256]{1,0:T(8,128)(2,1)S(1)}, bf16[128,256]{1,0:T(8,128)(2,1)}, u32[]{:S(2)}) copy-start(bf16[128,256]{1,0:T(8,128)(2,1)} %param.10) | copy-start | bytes 196612
  51.0 37.6 %all-to-all-start.2 = ((bf16[128,5,256]{2,1,0:T(8,128)(2,1)}), bf16[128,5,256]{2,1,0:T(8,128)(2,1)}, u32[]{:S(2)}, u32[]{:S(2)}) async-start(bf16[128,5,256]{2,1,0:T(8,128)(2,1)} %bitcast.4), calls=%async_computation.2 | async-start | bytes 1048576 | tf_op jit(solution)/shard_map/all_to_all | solution.py:97
  90.2 11.1 %copy-start.9 = (f32[1024]{0:T(1024)S(1)}, f32[1024]{0:T(1024)}, u32[]{:S(2)}) copy-start(f32[1024]{0:T(1024)} %param.17) | copy-start | bytes 12292
  90.2 179.8 %all-to-all-start.1 = ((bf16[128,5,1024]{2,1,0:T(8,128)(2,1)}), bf16[128,5,1024]{2,1,0:T(8,128)(2,1)S(1)}, u32[]{:S(2)}, u32[]{:S(2)}) async-start(bf16[128,5,1024]{2,1,0:T(8,128)(2,1)} %bitcast.75), calls=%async_computation.1 | async-start | bytes 4194304 | tf_op jit(solution)/shard_map/all_to_all | solution.py:104
  99.3 165.8 %all-gather.5.cloned.1.call-start = ((), (), s32[]{:S(2)}) async-start(), calls=%async_computation.8 | async-start | bytes 1638400 | tf_op jit(solution)/shard_map/all_gather | solution.py:113
  101.3 259.7 %reduce-scatter.2.cloned.1.call-start = ((), (), s32[]{:S(2)}) async-start(), calls=%async_computation.9 | async-start | bytes 1056768 | tf_op jit(solution)/shard_map/reduce_scatter | solution.py:63
  102.7 2.4 copy-start.10
  265.1 3.2 copy-start.4
  265.1 3.2 copy-start.11
  274.5 23.5 %copy-start.6 = (bf16[640,352]{0,1:T(8,128)(2,1)}, bf16[640,352]{0,1:T(8,128)(2,1)S(1)}, u32[]{:S(2)}) copy-start(bf16[640,352]{0,1:T(8,128)(2,1)S(1)} %get-tuple-element.59) | copy-start | bytes 1351684
  290.1 10.2 %all-to-all-start.5 = ((f32[2,1,320]{2,1,0:T(1,128)}), f32[2,1,320]{2,1,0:T(1,128)S(1)}, u32[]{:S(2)}, u32[]{:S(2)}) async-start(f32[2,1,320]{2,1,0:T(1,128)} %reshape.331), calls=%async_computation.5 | async-start | bytes 6144 | tf_op jit(solution)/shard_map/all_to_all | solution.py:29
  297.1 1.1 copy-start.5
  300.3 21.5 %all-to-all-start.3 = ((bf16[640,4,256]{2,0,1:T(8,128)(2,1)}), bf16[640,4,256]{2,0,1:T(8,128)(2,1)S(1)}, u32[]{:S(2)}, u32[]{:S(2)}) async-start(bf16[640,4,256]{2,0,1:T(8,128)(2,1)} %bitcast.77), calls=%async_computation.3 | async-start | bytes 2621440 | tf_op jit(solution)/shard_map/all_to_all | solution.py:149
  321.8 24.4 %all-to-all-start.6 = ((f32[64,2,5]{2,1,0:T(2,128)}), f32[64,2,5]{2,1,0:T(2,128)S(1)}, u32[]{:S(2)}, u32[]{:S(2)}) async-start(f32[64,2,5]{2,1,0:T(2,128)} %copy.76), calls=%async_computation.6 | async-start | bytes 131072 | tf_op jit(solution)/shard_map/all_to_all | solution.py:29
  346.2 38.7 %all-to-all-start.4 = ((bf16[128,5,256]{2,1,0:T(8,128)(2,1)}), bf16[128,5,256]{2,1,0:T(8,128)(2,1)S(1)}, u32[]{:S(2)}, u32[]{:S(2)}) async-start(bf16[128,5,256]{2,1,0:T(8,128)(2,1)} %all_to_all.54), calls=%async_computation.4 | async-start | bytes 1048576 | tf_op jit(solution)/shard_map/all_to_all | solution.py:155
  362.9 3.1 copy-start.7
  362.9 3.1 copy-start.12
  362.9 4.7 %copy-start.14 = (f32[640,352]{0,1:T(8,128)S(1)}, f32[640,352]{0,1:T(8,128)}, u32[]{:S(2)}) copy-start(f32[640,352]{0,1:T(8,128)} %fusion.11) | copy-start | bytes 2703364
  366.0 1.6 copy-start.3
  366.0 1.6 copy-start.13
  385.0 1.6 copy-start.2
Sparse Core Ops, SparseCore 0:
  102.8 34.8 all-gather.4
Sparse Core Ops, SparseCore 1:
  106.3 254.6 reduce-scatter.1
where the time goes:
time: 397 us; the launch traced here: 395 us
  blocking collectives  181 us (46%)
  waiting for transfers between devices  78.3 us (20%)
  starting transfers between devices  64.2 us (16%)
  local copies, waits for them, and re-layouts  31.7 us (8%)
  matrix products  19.6 us (5%)
  between operations  16 us (4%)
    all_gather x3, blocking collectives, stacked_from(): pieces = lax.all_gather(pieces, axes[k])  113 us
    psum x3, blocking collectives, over_axes(): return functools.reduce(lax.psum, axes, value)  42.1 us
    all_to_all x1, starting transfers between devices, local(): lax.all_to_all(weight_out, EP, split_axis=0, concat_axis=0, tiled=True)  20.4 us
    all_to_all x2, starting transfers between devices, exchange_in_order(): lax.all_to_all(pieces, axes[k], split_axis=k, concat_axis=k, tiled=True)  17.1 us
    all_to_all x1, waiting for transfers between devices, local(): lax.all_to_all(spread(jnp.take(tokens, token_of, axis=0), experts, group_...  16.9 us
    all_to_all x1, waiting for transfers between devices, local(): lax.all_to_all(partial_value, 'tp', split_axis=1, concat_axis=0, tiled=True)  15.8 us
    psum x1, blocking collectives, local(): route_sum = lax.psum(route_part, 'tp')  14.6 us
    all_to_all x2, waiting for transfers between devices, exchange_in_order(): lax.all_to_all(pieces, axes[k], split_axis=k, concat_axis=k, tiled=True)  13 us
  transfers between devices with their start and end apart: 9, of which 6 were waited for; matrix products, arithmetic and copies ran while one was open for 10% of the time, Pallas kernels for 0%

commit v1 on v0

v1 whole, which is shorter than its diff:
```python
import jax
import jax.numpy as jnp
from jax import lax
from jax.experimental import pallas as pl
from jax.experimental.pallas import tpu as pltpu
from jax.sharding import Mesh
from jax.sharding import PartitionSpec as P

EP = ("z", "x", "c")
MESH = pl.DeviceIdType.MESH
BF = jnp.bfloat16
F32 = jnp.float32
NZ = 16
NX = 4
NC = 2
NY = 4
CAP = 5
EXPERTS = NZ * NX
HK = NZ // NC
NQ = NX * NC
BLK = NQ * CAP
Z_ORDER = (0, 1, 7, 2, 6, 3, 5, 4)


def rdma(src, dst, send, recv, device):
    return pltpu.make_async_remote_copy(
        src_ref=src, dst_ref=dst, send_sem=send, recv_sem=recv, device_id=device, device_id_type=MESH
    )


def where_am_i():
    return tuple(lax.axis_index(a) for a in ("z", "x", "c", "y"))


def enter():
    z, x, c, y = where_am_i()
    barrier = pltpu.get_barrier_semaphore()

    def greet(device):
        pl.semaphore_signal(barrier, inc=1, device_id=device, device_id_type=MESH)

    for step in range(1, NQ):
        other = lax.rem(c * NX + x + step, NQ)
        greet((z, lax.rem(other, NX), other // NX, y))
    for step in range(1, NZ):
        greet((lax.rem(z + step, NZ), x, c, y))
    for step in range(1, NY):
        greet((z, x, c, lax.rem(y + step, NY)))
    pl.semaphore_wait(barrier, NQ - 1 + NZ - 1 + NY - 1)


def cols(index, width):
    return pl.ds(pl.multiple_of(index * width, width), width)


def permuted(perm_ref, value_ref, out_ref):
    width = value_ref.shape[-1]
    flat = value_ref[...].reshape(NQ * BLK, width)
    moved = jnp.dot(perm_ref[...], flat, preferred_element_type=F32).astype(BF)
    out_ref[...] = moved.reshape(NQ, BLK, width)


def dispatch_kernel(
    tok_ref, cot_slot_ref, cot_ref, wt_ref, perm_ref,
    rows_ref, grads_ref, full_ref, dense_ref,
    x_tok, x_cot, p_tok, p_cot,
    local_sem, x_send, x_recv, z_send, z_recv, yp_send, yp_recv, ym_send, ym_recv, f_send, f_recv,
    c_send, c_recv, g_send, g_recv, dz_send, dz_recv, dx_send, dx_recv, dc_send, dc_recv,
):
    z, x, c, y = where_am_i()
    width = tok_ref.shape[-1]
    me_q = c * NX + x
    y_up, y_down = lax.rem(y + 1, NY), lax.rem(y + NY - 1, NY)
    y_far = lax.rem(y + 2, NY)
    partner = (z, x, 1 - c, y)
    slots = (tok_ref, cot_slot_ref)
    gathered = (x_tok, x_cot)
    sorted_rows = (p_tok, p_cot)
    outs = (rows_ref, grads_ref)

    own = [
        pltpu.make_async_copy(tok_ref.at[me_q], x_tok.at[me_q], local_sem.at[0]),
        pltpu.make_async_copy(cot_slot_ref.at[me_q], x_cot.at[me_q], local_sem.at[1]),
        pltpu.make_async_copy(cot_ref, full_ref.at[:, cols(y, width)], local_sem.at[2]),
        pltpu.make_async_copy(wt_ref, dense_ref.at[z, x, c], local_sem.at[3]),
    ]
    for copy in own:
        copy.start()
    enter()

    def x_copy(a, step):
        other = lax.rem(me_q + step, NQ)
        return rdma(
            slots[a].at[other], gathered[a].at[me_q], x_send.at[a, step], x_recv.at[a, step],
            (z, lax.rem(other, NX), other // NX, y),
        )

    def x_arrival(a, step):
        source = lax.rem(me_q + NQ - step, NQ)
        return rdma(
            slots[a].at[source], gathered[a].at[source], x_send.at[a, step], x_recv.at[a, step],
            (z, lax.rem(source, NX), source // NX, y),
        )

    for a in range(2):
        for step in range(1, NQ):
            x_copy(a, step).start()

    def g_copy(step):
        return rdma(
            cot_ref, full_ref.at[:, cols(y, width)], g_send.at[step], g_recv.at[step],
            (z, x, c, lax.rem(y + step, NY)),
        )

    def g_arrival(step):
        source = lax.rem(y + NY - step, NY)
        return rdma(
            cot_ref, full_ref.at[:, cols(source, width)], g_send.at[step], g_recv.at[step],
            (z, x, c, source),
        )

    for step in range(1, NY):
        g_copy(step).start()

    def dz_copy(step):
        return rdma(
            wt_ref, dense_ref.at[z, x, c], dz_send.at[step], dz_recv.at[step],
            (lax.rem(z + step, NZ), x, c, y),
        )

    def dz_arrival(step):
        source = lax.rem(z + NZ - step, NZ)
        return rdma(
            wt_ref, dense_ref.at[source, x, c], dz_send.at[step], dz_recv.at[step], (source, x, c, y)
        )

    @pl.loop(1, NZ)
    def _(step):
        dz_copy(step).start()

    def z_copy(a, k):
        target = lax.rem(z + 2 * k + c, NZ)
        return rdma(
            sorted_rows[a].at[k], outs[a].at[c * HK + k, :, cols(y, width)],
            z_send.at[a, k], z_recv.at[a, k], (target, x, c, y),
        )

    def z_home(a):
        return pltpu.make_async_copy(
            sorted_rows[a].at[0], outs[a].at[0, :, cols(y, width)], local_sem.at[4 + a]
        )

    for a in range(2):
        own[a].wait()
        for step in range(1, NQ):
            x_arrival(a, step).wait_recv()
        permuted(perm_ref, gathered[a], sorted_rows[a])
        for k in Z_ORDER:
            if k == 0:

                @pl.when(c == 0)
                def _():
                    z_home(a).start()

                @pl.when(c == 1)
                def _():
                    z_copy(a, 0).start()
            else:
                z_copy(a, k).start()

    def y_copy(a, k, up):
        part = outs[a].at[c * HK + k, :, cols(y, width)]
        if up:
            return rdma(part, part, yp_send.at[a, k], yp_recv.at[a, k], (z, x, c, y_up))
        return rdma(part, part, ym_send.at[a, k], ym_recv.at[a, k], (z, x, c, y_down))

    def y_arrival(a, k, up):
        if up:
            part = outs[a].at[c * HK + k, :, cols(y_down, width)]
            return rdma(part, part, yp_send.at[a, k], yp_recv.at[a, k], (z, x, c, y_down))
        part = outs[a].at[c * HK + k, :, cols(y_up, width)]
        return rdma(part, part, ym_send.at[a, k], ym_recv.at[a, k], (z, x, c, y_up))

    def f_copy(a, k):
        source, target = (y_down, y_up) if k % 2 == 0 else (y_up, y_down)
        part = outs[a].at[c * HK + k, :, cols(source, width)]
        return rdma(part, part, f_send.at[a, k], f_recv.at[a, k], (z, x, c, target))

    def f_arrival(a, k):
        part = outs[a].at[c * HK + k, :, cols(y_far, width)]
        return rdma(part, part, f_send.at[a, k], f_recv.at[a, k], (z, x, c, y_up))

    def c_copy(a, k):
        block = outs[a].at[c * HK + k]
        return rdma(block, block, c_send.at[a, k], c_recv.at[a, k], partner)

    def c_arrival(a, k):
        block = outs[a].at[(1 - c) * HK + k]
        return rdma(block, block, c_send.at[a, k], c_recv.at[a, k], partner)

    def dx_copy(step):
        part = dense_ref.at[:, x, c]
        return rdma(part, part, dx_send.at[step], dx_recv.at[step], (z, lax.rem(x + step, NX), c, y))

    def dx_arrival(step):
        source = lax.rem(x + NX - step, NX)
        part = dense_ref.at[:, source, c]
        return rdma(part, part, dx_send.at[step], dx_recv.at[step], (z, source, c, y))

    def dc_copy(core):
        part = dense_ref.at[:, :, core]
        return rdma(part, part, dc_send.at[0], dc_recv.at[0], partner)

    order = [(a, k) for a in range(2) for k in Z_ORDER]
    for i in range(len(order) + 2):
        if i < len(order):
            a, k = order[i]
            if k == 0:

                @pl.when(c == 0)
                def _():
                    z_home(a).wait()

                @pl.when(c == 1)
                def _():
                    z_copy(a, 0).wait_recv()
            else:
                z_copy(a, k).wait_recv()
            y_copy(a, k, True).start()
            y_copy(a, k, False).start()
        if 1 <= i <= len(order):
            a, k = order[i - 1]
            up = k % 2 == 0
            y_arrival(a, k, up).wait_recv()
            f_copy(a, k).start()
            y_arrival(a, k, not up).wait_recv()
        if i >= 2:
            a, k = order[i - 2]
            f_arrival(a, k).wait_recv()
            c_copy(a, k).start()
        if i == 6:
            own[3].wait()

            @pl.loop(1, NZ)
            def _(step):
                dz_arrival(step).wait_recv()

            for step in range(1, NX):
                dx_copy(step).start()
        if i == 10:
            for step in range(1, NX):
                dx_arrival(step).wait_recv()
            dc_copy(c).start()

    own[2].wait()
    for step in range(1, NY):
        g_arrival(step).wait_recv()
    dc_copy(1 - c).wait_recv()
    for a, k in order:
        c_arrival(a, k).wait_recv()
    for a in range(2):
        for step in range(1, NQ):
            x_copy(a, step).wait_send()
    for step in range(1, NY):
        g_copy(step).wait_send()

    @pl.loop(1, NZ)
    def _(step):
        dz_copy(step).wait_send()

    for step in range(1, NX):
        dx_copy(step).wait_send()
    dc_copy(c).wait_send()
    for a, k in order:
        if k == 0:

            @pl.when(c == 1)
            def _():
                z_copy(a, 0).wait_send()
        else:
            z_copy(a, k).wait_send()
        y_copy(a, k, True).wait_send()
        y_copy(a, k, False).wait_send()
        f_copy(a, k).wait_send()
        c_copy(a, k).wait_send()


def combine_kernel(
    part_ref, aux_ref, moment_ref, gain_ref, perm_ref,
    out_ref, aux_out, moment_out, gain_out,
    p_in, aux_in, m_in, g_in,
    first, first_in, second_in, back, back_in, sorted_back,
    aux_sum, aux_y, aux_z, aux_t,
    m_half, m_x, m_xsum, m_z, g_sum, g_x, g_sum2, g_y, g_sum3, g_z,
    local_sem, d_send, d_recv, b1_send, b1_recv, b2_send, b2_recv, ay_send, ay_recv,
    z_send, z_recv, za_send, za_recv, x_send, x_recv, xa_send, xa_recv,
    mx_send, mx_recv, mz_send, mz_recv, gx_send, gx_recv, gy_send, gy_recv, gz_send, gz_recv,
):
    z, x, c, y = where_am_i()
    width = out_ref.shape[-1]
    half = HK // 2
    me_q = c * NX + x
    partner = (z, x, 1 - c, y)
    flip1 = y + 1 - 2 * lax.rem(y, 2)
    flip3 = NY - 1 - y
    flip2 = lax.rem(y + 2, NY)
    pairs = ((flip1, flip3), (flip3, flip1))

    enter()
    d_copies = [
        rdma(part_ref.at[pl.ds((1 - c) * HK, HK)], p_in, d_send.at[0], d_recv.at[0], partner),
        rdma(aux_ref.at[pl.ds((1 - c) * HK, HK)], aux_in, d_send.at[1], d_recv.at[1], partner),
        rdma(gain_ref, g_in, d_send.at[2], d_recv.at[2], partner),
        rdma(moment_ref.at[:, :, 1 - c], m_in, d_send.at[3], d_recv.at[3], partner),
    ]
    for copy in d_copies:
        copy.start()

    d_copies[0].wait_recv()

    def b1_copy(h):
        return rdma(
            first.at[h, pl.ds(2, 2)], first_in.at[h], b1_send.at[h], b1_recv.at[h],
            (z, x, c, pairs[h][0]),
        )

    def both(h, i, owner):
        for j in range(half):
            mine = part_ref[c * HK + h * half + j, :, cols(owner, width)].astype(F32)
            theirs = p_in[h * half + j, :, cols(owner, width)].astype(F32)
            first[h, i, j] = (mine + theirs).astype(BF)

    for h in range(2):
        both(h, 2, pairs[h][0])
        both(h, 3, flip2)
        b1_copy(h).start()
    for h in range(2):
        both(h, 0, y)
        both(h, 1, pairs[h][1])

    d_copies[1].wait_recv()
    aux_sum[...] = aux_ref[pl.ds(c * HK, HK)] + aux_in[...]

    def ay_copy(step):
        return rdma(aux_sum, aux_y.at[y], ay_send.at[step], ay_recv.at[step],
                    (z, x, c, lax.rem(y + step, NY)))

    def ay_arrival(step):
        source = lax.rem(y + NY - step, NY)
        return rdma(aux_sum, aux_y.at[source], ay_send.at[step], ay_recv.at[step], (z, x, c, source))

    for step in range(1, NY):
        ay_copy(step).start()
    aux_y[y] = aux_sum[...]

    d_copies[2].wait_recv()
    g_sum[...] = gain_ref[...] + g_in[...]
    g_x[x] = g_sum[...]

    def gx_copy(step):
        return rdma(g_sum, g_x.at[x], gx_send.at[step], gx_recv.at[step],
                    (z, lax.rem(x + step, NX), c, y))

    def gx_arrival(step):
        source = lax.rem(x + NX - step, NX)
        return rdma(g_sum, g_x.at[source], gx_send.at[step], gx_recv.at[step], (z, source, c, y))

    for step in range(1, NX):
        gx_copy(step).start()

    d_copies[3].wait_recv()
    for i in range(NX):
        m_half[:, i] = moment_ref[:, i, c] + m_in[:, i]

    def mx_copy(step):
        other = lax.rem(x + step, NX)
        return rdma(m_half.at[:, other], m_x.at[step - 1], mx_send.at[step], mx_recv.at[step],
                    (z, other, c, y))

    for step in range(1, NX):
        mx_copy(step).start()

    def b2_copy(h):
        return rdma(first.at[h, 3], second_in.at[h], b2_send.at[h], b2_recv.at[h],
                    (z, x, c, pairs[h][1]))

    for h in range(2):
        b1_copy(h).wait()
        first[h, 3] = (first[h, 1].astype(F32) + first_in[h, 1].astype(F32)).astype(BF)
        b2_copy(h).start()

    for step in range(1, NX):
        gx_arrival(step).wait_recv()
    g_sum2[...] = g_x[0] + g_x[1] + g_x[2] + g_x[3]
    g_y[y] = g_sum2[...]

    def gy_copy(step):
        return rdma(g_sum2, g_y.at[y], gy_send.at[step], gy_recv.at[step],
                    (z, x, c, lax.rem(y + step, NY)))

    def gy_arrival(step):
        source = lax.rem(y + NY - step, NY)
        return rdma(g_sum2, g_y.at[source], gy_send.at[step], gy_recv.at[step], (z, x, c, source))

    for step in range(1, NY):
        gy_copy(step).start()

    for step in range(1, NX):
        mx_copy(step).wait_recv()
    m_xsum[...] = m_half[:, x] + m_x[0] + m_x[1] + m_x[2]

    def mz_copy(step):
        other = lax.rem(z + step, NZ)
        return rdma(m_xsum.at[other], m_z.at[step], mz_send.at[step], mz_recv.at[step],
                    (other, x, c, y))

    @pl.loop(1, NZ)
    def _(step):
        mz_copy(step).start()

    for step in range(1, NY):
        ay_arrival(step).wait_recv()
        ay_copy(step).wait_send()
    aux_sum[...] = aux_y[0] + aux_y[1] + aux_y[2] + aux_y[3]

    def z_copy(k):
        target = lax.rem(z + 2 * NZ - 2 * k - c, NZ)
        return rdma(back.at[k], back_in.at[k], z_send.at[k], z_recv.at[k], (target, x, c, y))

    def za_copy(k):
        target = lax.rem(z + 2 * NZ - 2 * k - c, NZ)
        return rdma(aux_sum.at[k], aux_z.at[k], za_send.at[k], za_recv.at[k], (target, x, c, y))

    z_home = [
        pltpu.make_async_copy(back.at[0], back_in.at[0], local_sem.at[0]),
        pltpu.make_async_copy(aux_sum.at[0], aux_z.at[0], local_sem.at[1]),
    ]

    def send_back(k):
        if k == 0:

            @pl.when(c == 0)
            def _():
                z_home[0].start()
                z_home[1].start()

            @pl.when(c == 1)
            def _():
                z_copy(0).start()
                za_copy(0).start()
        else:
            z_copy(k).start()
            za_copy(k).start()

    for h in range(2):
        b2_copy(h).wait()
        back[pl.ds(h * half, half)] = (
            first[h, 0].astype(F32) + first_in[h, 0].astype(F32) + second_in[h].astype(F32)
        ).astype(BF)
    for k in reversed(Z_ORDER):
        send_back(k)

    for step in range(1, NY):
        gy_arrival(step).wait_recv()
    g_sum3[...] = g_y[0] + g_y[1] + g_y[2] + g_y[3]
    g_z[z] = g_sum3[...]

    def gz_copy(step):
        return rdma(g_sum3, g_z.at[z], gz_send.at[step], gz_recv.at[step],
                    (lax.rem(z + step, NZ), x, c, y))

    def gz_arrival(step):
        source = lax.rem(z + NZ - step, NZ)
        return rdma(g_sum3, g_z.at[source], gz_send.at[step], gz_recv.at[step], (source, x, c, y))

    @pl.loop(1, NZ)
    def _(step):
        gz_copy(step).start()

    for k in Z_ORDER:
        if k == 0:

            @pl.when(c == 0)
            def _():
                z_home[0].wait()
                z_home[1].wait()

            @pl.when(c == 1)
            def _():
                z_copy(0).wait()
                za_copy(0).wait()
        else:
            z_copy(k).wait()
            za_copy(k).wait()
    permuted(perm_ref, back_in, sorted_back)
    for q in range(NQ):
        aux_t[q] = aux_z[:, q, :]

    def x_copy(step):
        other = lax.rem(me_q + step, NQ)
        return rdma(sorted_back.at[other], out_ref.at[me_q], x_send.at[step], x_recv.at[step],
                    (z, lax.rem(other, NX), other // NX, y))

    def xa_copy(step):
        other = lax.rem(me_q + step, NQ)
        return rdma(aux_t.at[other], aux_out.at[me_q], xa_send.at[step], xa_recv.at[step],
                    (z, lax.rem(other, NX), other // NX, y))

    def x_arrival(step):
        source = lax.rem(me_q + NQ - step, NQ)
        device = (z, lax.rem(source, NX), source // NX, y)
        return (
            rdma(sorted_back.at[source], out_ref.at[source], x_send.at[step], x_recv.at[step], device),
            rdma(aux_t.at[source], aux_out.at[source], xa_send.at[step], xa_recv.at[step], device),
        )

    for step in range(1, NQ):
        x_copy(step).start()
        xa_copy(step).start()
    out_ref[me_q] = sorted_back[me_q]
    aux_out[me_q] = aux_t[me_q]

    m_z[0] = m_xsum[z]

    @pl.loop(1, NZ)
    def _(step):
        mz_copy(step).wait()
        gz_arrival(step).wait_recv()
        gz_copy(step).wait_send()

    moment_out[...] = jnp.sum(m_z[...], axis=0)
    gain_out[...] = jnp.sum(g_z[...], axis=0)

    for step in range(1, NQ):
        for arrival in x_arrival(step):
            arrival.wait_recv()
        x_copy(step).wait_send()
        xa_copy(step).wait_send()
    for copy in d_copies:
        copy.wait_send()
    for step in range(1, NX):
        gx_copy(step).wait_send()
        mx_copy(step).wait_send()
    for step in range(1, NY):
        gy_copy(step).wait_send()


VMEM_SPEC = pl.BlockSpec(memory_space=pltpu.VMEM)
DMA = pltpu.SemaphoreType.DMA


def dispatch(tok_slots, cot_slots, cotangent, wt, perm):
    width = cotangent.shape[1]
    return pl.pallas_call(
        dispatch_kernel,
        out_shape=(
            jax.ShapeDtypeStruct((NZ, BLK, NY * width), BF),
            jax.ShapeDtypeStruct((NZ, BLK, NY * width), BF),
            jax.ShapeDtypeStruct((cotangent.shape[0], NY * width), BF),
            jax.ShapeDtypeStruct((NZ, NX, NC) + wt.shape, BF),
        ),
        in_specs=[VMEM_SPEC] * 5,
        out_specs=(VMEM_SPEC,) * 4,
        scratch_shapes=[pltpu.VMEM((NQ, BLK, width), BF)] * 4
        + [
            DMA((6,)),
            DMA((2, NQ)), DMA((2, NQ)),
            DMA((2, HK)), DMA((2, HK)),
            DMA((2, HK)), DMA((2, HK)),
            DMA((2, HK)), DMA((2, HK)),
            DMA((2, HK)), DMA((2, HK)),
            DMA((2, HK)), DMA((2, HK)),
            DMA((NY,)), DMA((NY,)),
            DMA((NZ,)), DMA((NZ,)),
            DMA((NX,)), DMA((NX,)),
            DMA((1,)), DMA((1,)),
        ],
        compiler_params=pltpu.CompilerParams(collective_id=0, has_side_effects=True),
        name="dispatch",
    )(tok_slots, cot_slots, cotangent, wt, perm)


def combine(partial, aux, moment, gain, perm):
    width = partial.shape[2] // NY
    half = HK // 2
    lanes = aux.shape[2]
    own, feats = moment.shape[3:]
    g = gain.shape
    vm = pltpu.VMEM
    return pl.pallas_call(
        combine_kernel,
        out_shape=(
            jax.ShapeDtypeStruct((NQ, BLK, width), BF),
            jax.ShapeDtypeStruct((NQ, HK, lanes), F32),
            jax.ShapeDtypeStruct((own, feats), F32),
            jax.ShapeDtypeStruct(g, F32),
        ),
        in_specs=[VMEM_SPEC] * 5,
        out_specs=(VMEM_SPEC,) * 4,
        scratch_shapes=[
            vm((HK, BLK, NY * width), BF),
            vm((HK, NQ, lanes), F32),
            vm((NZ, NX, own, feats), F32),
            vm(g, F32),
            vm((2, NY, half, BLK, width), BF),
            vm((2, 2, half, BLK, width), BF),
            vm((2, half, BLK, width), BF),
            vm((HK, BLK, width), BF),
            vm((HK, BLK, width), BF),
            vm((NQ, BLK, width), BF),
            vm((HK, NQ, lanes), F32),
            vm((NY, HK, NQ, lanes), F32),
            vm((HK, NQ, lanes), F32),
            vm((NQ, HK, lanes), F32),
            vm((NZ, NX, own, feats), F32),
            vm((NX - 1, NZ, own, feats), F32),
            vm((NZ, own, feats), F32),
            vm((NZ, own, feats), F32),
            vm(g, F32),
            vm((NX,) + g, F32),
            vm(g, F32),
            vm((NY,) + g, F32),
            vm(g, F32),
            vm((NZ,) + g, F32),
            DMA((2,)),
            DMA((4,)), DMA((4,)),
            DMA((2,)), DMA((2,)),
            DMA((2,)), DMA((2,)),
            DMA((NY,)), DMA((NY,)),
            DMA((HK,)), DMA((HK,)),
            DMA((HK,)), DMA((HK,)),
            DMA((NQ,)), DMA((NQ,)),
            DMA((NQ,)), DMA((NQ,)),
            DMA((NX,)), DMA((NX,)),
            DMA((NZ,)), DMA((NZ,)),
            DMA((NX,)), DMA((NX,)),
            DMA((NY,)), DMA((NY,)),
            DMA((NZ,)), DMA((NZ,)),
        ],
        compiler_params=pltpu.CompilerParams(collective_id=1, has_side_effects=True),
        name="combine",
    )(partial, aux, moment, gain, perm)


def local(tokens, cotangent, routes, route_weights, w_gate, w_up, w_down, dense_weight, mix_gate):
    z, x, c = (lax.axis_index(a) for a in EP)
    token_count = routes.shape[0]
    ep_count = NZ * NX * NC
    e = jnp.arange(EXPERTS, dtype=jnp.int32)
    expert = lax.rem(z + 2 * lax.rem(e, HK) + e // (HK * NX), NZ) * NX + lax.rem(e // HK, NX)
    picked = routes.T
    hits = [picked[p][None, :] == expert[:, None] for p in range(2)]
    hit = hits[0] | hits[1]
    t = jnp.arange(token_count, dtype=jnp.int32)
    earlier = (t[:, None] < t[None, :]).astype(BF)
    rank = jnp.dot(hit.astype(BF), earlier, preferred_element_type=F32).astype(jnp.int32)
    s = jnp.arange(CAP, dtype=jnp.int32)
    chosen = (hit[:, None, :] & (rank[:, None, :] == s[None, :, None])).reshape(-1, token_count)
    weights = route_weights.T
    weight = jnp.where(hits[0], weights[0][None, :], weights[1][None, :])
    weight = jnp.broadcast_to(weight[:, None, :], (EXPERTS, CAP, token_count)).reshape(-1, token_count)
    select = chosen.astype(BF)
    select_weighted = jnp.where(chosen, weight, jnp.zeros_like(weight))
    tok_slots = jnp.dot(select, tokens, preferred_element_type=F32).astype(BF).reshape(NQ, BLK, -1)
    cot_slots = (
        jnp.dot(select_weighted, cotangent, preferred_element_type=F32).astype(BF).reshape(NQ, BLK, -1)
    )
    r = jnp.arange(NQ * BLK, dtype=jnp.int32)
    moved = lax.rem(r, BLK) // CAP * BLK + r // BLK * CAP + lax.rem(r, CAP)
    perm = (moved[:, None] == r[None, :]).astype(BF)
    rows_in, grads_in, cot_full, wt_full = dispatch(
        tok_slots, cot_slots, cotangent, dense_weight.T, perm
    )

    rows_in = rows_in.reshape(NZ * BLK, -1)
    grads_in = grads_in.reshape(NZ * BLK, -1)
    wt_full = wt_full.reshape(ep_count * dense_weight.shape[1], -1)
    gate_matrix, up_matrix, down_matrix = w_gate[0], w_up[0], w_down[0]
    rows_by = (((0,), (0,)), ((), ()))
    cols_by = (((1,), (1,)), ((), ()))

    def dot(a, b, dims):
        return lax.dot_general(a, b, dims, preferred_element_type=F32)

    pre_gate = jnp.dot(rows_in, gate_matrix, preferred_element_type=F32)
    pre_up = jnp.dot(rows_in, up_matrix, preferred_element_type=F32)
    back = dot(grads_in, down_matrix, cols_by)
    sig = jax.nn.sigmoid(pre_gate)
    act = pre_gate * sig
    hidden_bf = (act * pre_up).astype(BF)
    route_part = jnp.sum(hidden_bf.astype(F32) * back, axis=1)
    d_gate = (back * pre_up * sig * (1.0 + pre_gate * (1.0 - sig))).astype(BF)
    d_up = (back * act).astype(BF)
    partial = (dot(d_gate, gate_matrix, cols_by) + dot(d_up, up_matrix, cols_by)).astype(BF)
    aux = jnp.pad(route_part.reshape(NZ, NQ, CAP), ((0, 0), (0, 0), (0, 128 - CAP)))
    moment = dot(cot_full, tokens, rows_by)
    gain = jnp.sum(wt_full.astype(F32) * moment, axis=1).reshape(-1, 128)
    own = dense_weight.shape[1]
    slots, aux_back, moment_own, gain_all = combine(
        partial.reshape(NZ, BLK, -1), aux, moment.reshape(NZ, NX, NC, own, -1), gain, perm
    )

    gate_grad = dot(rows_in, d_gate, rows_by).astype(BF)[None]
    up_grad = dot(rows_in, d_up, rows_by).astype(BF)[None]
    down_grad = dot(hidden_bf, grads_in, rows_by).astype(BF)[None]
    scaled = (mix_gate[None, :] * cot_full.astype(F32)).astype(BF)
    dense_dx = jnp.dot(scaled, wt_full, preferred_element_type=F32)
    token_grad = (dense_dx + dot(select, slots.reshape(NQ * BLK, -1), rows_by)).astype(BF)
    values = aux_back[:, :, :CAP].reshape(EXPERTS, CAP)
    at_slot = jnp.sum(
        jnp.where(rank[:, :, None] == s[None, None, :], values[:, None, :], 0.0), axis=2
    )
    route_sums = jnp.stack([jnp.sum(jnp.where(h, at_slot, 0.0), axis=0) for h in hits], axis=1)
    route_grad = route_sums / route_weights.astype(F32)
    ep_index = (z * NX + x) * NC + c
    own_gate = lax.dynamic_slice(mix_gate, (ep_index * own,), (own,))
    dense_grad = (moment_own * (own_gate[:, None] * (1.0 / ep_count))).T
    mix_grad = gain_all.reshape(-1) / ep_count
    return token_grad, route_grad, gate_grad, up_grad, down_grad, dense_grad, mix_grad


def solution(mesh):
    finer = Mesh(mesh.devices.reshape(NZ, NX, NC, NY), EP + ("y",))
    in_specs = (
        P(EP, "y"),
        P(EP, "y"),
        P(EP, None),
        P(EP, None),
        P(EP, None, "y"),
        P(EP, None, "y"),
        P(EP, "y", None),
        P("y", EP),
        P(),
    )
    out_specs = (
        P(EP, "y"),
        P(EP, None),
        P(EP, None, "y"),
        P(EP, None, "y"),
        P(EP, "y", None),
        P("y", EP),
        P(),
    )
    return jax.shard_map(local, mesh=finer, in_specs=in_specs, out_specs=out_specs, check_vma=False)
```

time: 397 us -> 137 us (0.35)
  blocking collectives: 181 us -> 0 us
  Pallas kernels: 0 us -> 111 us
  waiting for transfers between devices: 78.3 us -> 0 us
  starting transfers between devices: 64.2 us -> 0 us
  local copies, waits for them, and re-layouts: 31.7 us -> 4.3 us
  between operations: 16 us -> 0.92 us
    all_gather x4 -> x0, blocking collectives: 125 us -> none  [the longest x3 113 us: stacked_from(): pieces = lax.all_gather(pieces, axes[k])]
    pallas_call x0 -> x2, Pallas kernels: none -> 111 us  [the longest x1 66.8 us: dispatch(): pl.pallas_call(dispatch_kernel, out_shape=(jax.ShapeDtypeStruct((NZ, BLK,...]
    all_to_all x7 -> x0, waiting for transfers between devices: 70.8 us -> none  [the longest x1 16.9 us: local(): lax.all_to_all(spread(jnp.take(tokens, token_of, axis=0), experts, group_...]
    all_to_all x7 -> x0, starting transfers between devices: 64.1 us -> none  [the longest x1 20.4 us: local(): lax.all_to_all(weight_out, EP, split_axis=0, concat_axis=0, tiled=True)]
    psum x4 -> x0, blocking collectives: 56.7 us -> none  [the longest x3 42.1 us: over_axes(): return functools.reduce(lax.psum, axes, value)]
    gather x10 -> x0, local copies, waits for them, and re-layouts: 10.1 us -> none  [the longest x2 2.51 us: local(): jnp.take(route_weights.reshape(-1), pick_of, axis=0)]
    reduce_scatter x1 -> x0, waiting for transfers between devices: 7.46 us -> none  [own_tiles(): lax.psum_scatter(padded.reshape(-1, 128), axis, scatter_dimension=0, tile...]
    all_to_all x7 -> x0, local copies, waits for them, and re-layouts: 7.35 us -> none  [the longest x1 1.91 us: local(): lax.all_to_all(spread(jnp.take(tokens, token_of, axis=0), experts, group_...]
  transfers between devices with their start and end apart: 9 -> 0, of which waited for: 6 -> 0; matrix products, arithmetic and copies ran while one was open for 10% -> 0% of each run, Pallas kernels for 0% -> 0%
where the time goes in v1:
time: 137 us
  Pallas kernels  111 us (81%)
  matrix products  17.5 us (13%)
  local copies, waits for them, and re-layouts  4.3 us (3%)
  other arithmetic  3.29 us (2%)
    pallas_call x1, Pallas kernels, dispatch(): pl.pallas_call(dispatch_kernel, out_shape=(jax.ShapeDtypeStruct((NZ, BLK,...  66.8 us
    pallas_call x1, Pallas kernels, combine(): pl.pallas_call(combine_kernel, out_shape=(jax.ShapeDtypeStruct((NQ, BLK,...  44.2 us
    dot_general x8, matrix products, dot(): return lax.dot_general(a, b, dims, preferred_element_type=F32)  11.7 us

profile of v1, /device:TPU:1, one launch (start us, length us, event | category | flops | bytes accessed | tf_op | source)
XLA Modules:
  0.0 137.0 jit_solution(5230769950764797024)
XLA Ops:
  0.6 0.0 copy-start
  0.6 0.0 copy-start.4
  0.7 0.0 copy-start.5
  0.7 0.8 slice_bitcast_fusion.4
  1.5 0.2 convolution_convert_fusion.5
  1.7 0.0 copy-start.3
  1.7 0.1 compare_or_fusion
  1.9 0.1 eq.112
  2.1 0.1 compare_and_fusion
  2.2 0.7 slice_bitcast_fusion.2
  2.9 0.1 compare_select_fusion.1
  3.1 0.0 copy-done.4
  3.1 0.9 convolution_convert_fusion.3
  3.9 0.0 copy-done.5
  3.9 0.9 convolution_convert_fusion.4
  4.8 0.8 fusion.14.perm_ref
  5.6 66.8 %dispatch.1 = (bf16[16,40,1024]{2,1,0:T(8,128)(2,1)}, bf16[16,40,1024]{2,1,0:T(8,128)(2,1)}, bf16[128,1024]{1,0:T(8,128)(2,1)}, bf16[16,4,2,8,256]{4,3,2,1,0:T(8,128)(2,1)}) custom-call(bf16[8,40,256]{2,1,0:T(8,128)(2,1)} %bitcast.73, bf16[8,40,256]{2,1,0:T(8,128)(2,1)} %bitcast.72, bf16[128,256]{1,0:T(8,128)(2,1)} %cot_ref.1, bf16[8,256]{1,0:T(8,128)(2,1)} %bitcast.77, ...), custom_call_target="tpu_custom_call" | custom-call | tf_op jit(solution)/shard_map/dispatch/pallas_call | solution.py:554
  72.5 0.0 copy-done.3
  72.5 0.0 copy-start.10
  72.5 2.2 %fusion.10 = f32[640,352]{0,1:T(8,128)S(1)} fusion(bf16[640,1024]{1,0:T(8,128)(2,1)} %bitcast.81, bf16[1,1024,352]{1,2,0:T(8,128)(2,1)S(1)} %copy-done.3), kind=kOutput, calls=%fused_computation.24 | convolution fusion | flops 461373440 | bytes 2932736 | tf_op jit(solution)/shard_map/dot_general | solution.py:686
  74.7 0.0 copy-done
  74.7 0.0 copy-start.12
  74.7 0.8 fusion.7
  75.5 0.5 copy-done.11
  76.0 0.2 copy-done.12
  76.2 1.1 multiply_reduce_fusion.1
  77.2 1.6 %fusion = bf16[1,352,1024]{2,1,0:T(8,128)(2,1)} fusion(bf16[640,352]{0,1:T(8,128)(2,1)S(1)} %get-tuple-element.26, bf16[640,1024]{1,0:T(8,128)(2,1)S(1)} %bitcast.86), kind=kOutput, calls=%fused_computation.4 | convolution fusion | flops 461733888 | bytes 2482176 | tf_op jit(solution)/shard_map/dot_general | solution.py:683
  78.8 1.6 %fusion.1 = bf16[1,1024,352]{1,2,0:T(8,128)(2,1)} fusion(bf16[640,352]{0,1:T(8,128)(2,1)S(1)} %get-tuple-element.27, bf16[640,1024]{1,0:T(8,128)(2,1)S(1)} %bitcast.83), kind=kOutput, calls=%fused_computation.5 | convolution fusion | flops 461733888 | bytes 2482176 | tf_op jit(solution)/shard_map/dot_general | solution.py:683
  80.4 1.6 %fusion.2 = bf16[1,1024,352]{1,2,0:T(8,128)(2,1)} fusion(bf16[640,352]{0,1:T(8,128)(2,1)S(1)} %get-tuple-element.28, bf16[640,1024]{1,0:T(8,128)(2,1)S(1)} %bitcast.84), kind=kOutput, calls=%fused_computation.6 | convolution fusion | flops 461733888 | bytes 2482176 | tf_op jit(solution)/shard_map/dot_general | solution.py:683
  82.0 0.9 fusion.5
  82.9 2.0 %add_convert_fusion = bf16[640,1024]{1,0:T(8,128)(2,1)} fusion(f32[640,1024]{1,0:T(8,128)S(1)} %fusion.5, bf16[640,352]{0,1:T(8,128)(2,1)S(1)} %get-tuple-element.28, bf16[1,1024,352]{1,2,0:T(8,128)(2,1)S(1)} %copy-done.3), kind=kOutput, calls=%fused_computation | convolution fusion | flops 462684160 | bytes 5103616 | tf_op jit(solution)/shard_map/dot_general | solution.py:683
  84.9 1.9 %multiply_reduce_fusion = (f32[1024]{0:T(1024)}, f32[1024,256]{1,0:T(8,128)}) fusion(bf16[16,4,2,8,256]{4,3,2,1,0:T(8,128)(2,1)S(1)} %copy-done.1, bf16[128,1024]{1,0:T(8,128)(2,1)S(1)} %copy-done.2, bf16[128,256]{1,0:T(8,128)(2,1)S(1)} %copy-done.5), kind=kOutput, calls=%fused_computation.12 | convolution fusion | flops 67894272 | bytes 1904640 | tf_op jit(solution)/shard_map/dot_general | solution.py:683
  86.8 0.2 reshape.262
  87.0 0.6 pad.4.aux_ref
  87.6 44.2 %combine.1 = (bf16[8,40,256]{2,1,0:T(8,128)(2,1)}, f32[8,8,128]{2,1,0:T(8,128)}, f32[8,256]{1,0:T(8,128)}, f32[8,128]{1,0:T(8,128)}) custom-call(bf16[16,40,1024]{2,1,0:T(8,128)(2,1)} %bitcast.69, f32[16,8,128]{2,1,0:T(8,128)} %pad.4.aux_ref, f32[16,4,2,8,256]{4,3,2,1,0:T(8,128)} %bitcast.70, f32[8,128]{1,0:T(8,128)} %bitcast.75, ...), custom_call_target="tpu_custom_call" | custom-call | tf_op jit(solution)/shard_map/combine/pallas_call | solution.py:590
  131.9 0.8 slice_bitcast_fusion
  132.6 0.1 copy.16
  132.7 0.1 select_reduce_fusion
  132.8 0.1 fusion.20
  132.9 0.6 maximum_divide_fusion
  133.5 0.1 fusion.16
  133.6 1.2 fusion.40
  134.8 0.0 copy-done.8
  134.8 0.9 fusion.3
  135.7 0.1 dynamic-slice_multiply_fusion
  135.7 0.0 copy-done.6
  135.7 0.7 multiply_bitcast_fusion
  136.4 0.6 multiply_bitcast_fusion.1
  (22 shorter events, 0.3 us)
Async XLA Ops:
  0.6 74.0 %copy-start = (bf16[1,1024,352]{1,2,0:T(8,128)(2,1)S(1)}, bf16[1,1024,352]{1,2,0:T(8,128)(2,1)}, u32[]{:S(2)}) copy-start(bf16[1,1024,352]{1,2,0:T(8,128)(2,1)} %param.13) | copy-start | bytes 2162692
  0.6 2.4 %copy-start.4 = (bf16[128,256]{1,0:T(8,128)(2,1)S(1)}, bf16[128,256]{1,0:T(8,128)(2,1)}, u32[]{:S(2)}) copy-start(bf16[128,256]{1,0:T(8,128)(2,1)} %cot_ref.1) | copy-start | bytes 196612
  0.7 3.3 %copy-start.5 = (bf16[128,256]{1,0:T(8,128)(2,1)S(1)}, bf16[128,256]{1,0:T(8,128)(2,1)}, u32[]{:S(2)}) copy-start(bf16[128,256]{1,0:T(8,128)(2,1)} %param.9) | copy-start | bytes 196612
  1.7 70.7 %copy-start.3 = (bf16[1,1024,352]{1,2,0:T(8,128)(2,1)S(1)}, bf16[1,1024,352]{1,2,0:T(8,128)(2,1)}, u32[]{:S(2)}) copy-start(bf16[1,1024,352]{1,2,0:T(8,128)(2,1)} %param.14) | copy-start | bytes 2162692
  72.5 2.2 %copy-start.10 = (bf16[16,40,1024]{2,1,0:T(8,128)(2,1)S(1)}, bf16[16,40,1024]{2,1,0:T(8,128)(2,1)}, u32[]{:S(2)}) copy-start(bf16[16,40,1024]{2,1,0:T(8,128)(2,1)} %get-tuple-element.18) | copy-start | bytes 3932164
  74.7 1.3 copy-start.11
  74.7 1.5 %copy-start.12 = (bf16[1,352,1024]{2,1,0:T(8,128)(2,1)S(1)}, bf16[1,352,1024]{2,1,0:T(8,128)(2,1)}, u32[]{:S(2)}) copy-start(bf16[1,352,1024]{2,1,0:T(8,128)(2,1)} %param.15) | copy-start | bytes 2162692
  82.9 2.0 %copy-start.1 = (bf16[16,4,2,8,256]{4,3,2,1,0:T(8,128)(2,1)S(1)}, bf16[16,4,2,8,256]{4,3,2,1,0:T(8,128)(2,1)}, u32[]{:S(2)}) copy-start(bf16[16,4,2,8,256]{4,3,2,1,0:T(8,128)(2,1)} %get-tuple-element.16) | copy-start | bytes 1572868
  82.9 2.0 %copy-start.2 = (bf16[128,1024]{1,0:T(8,128)(2,1)S(1)}, bf16[128,1024]{1,0:T(8,128)(2,1)}, u32[]{:S(2)}) copy-start(bf16[128,1024]{1,0:T(8,128)(2,1)} %get-tuple-element.15) | copy-start | bytes 786436
  87.6 45.3 %copy-start.7 = (bf16[128,2]{0,1:T(2,128)(2,1)S(1)}, bf16[128,2]{0,1:T(2,128)(2,1)}, u32[]{:S(2)}) copy-start(bf16[128,2]{0,1:T(2,128)(2,1)} %param.12) | copy-start | bytes 1540
  87.6 47.1 %copy-start.8 = (f32[1024]{0:T(1024)S(1)}, f32[1024]{0:T(1024)}, u32[]{:S(2)}) copy-start(f32[1024]{0:T(1024)} %param.17) | copy-start | bytes 12292
  131.8 3.9 %copy-start.6 = (f32[8,256]{1,0:T(8,128)S(1)}, f32[8,256]{1,0:T(8,128)}, u32[]{:S(2)}) copy-start(f32[8,256]{1,0:T(8,128)} %get-tuple-element.21) | copy-start | bytes 24580
  131.8 4.6 %copy-start.9 = (f32[8,128]{1,0:T(8,128)S(1)}, f32[8,128]{1,0:T(8,128)}, u32[]{:S(2)}) copy-start(f32[8,128]{1,0:T(8,128)} %get-tuple-element.22) | copy-start | bytes 12292

commit v2 on v1

v2 whole, which is shorter than its diff:
```python
import jax
import jax.numpy as jnp
from jax import lax
from jax.experimental import pallas as pl
from jax.experimental.pallas import tpu as pltpu
from jax.sharding import Mesh
from jax.sharding import PartitionSpec as P

EP = ("z", "x", "c")
MESH = pl.DeviceIdType.MESH
BF = jnp.bfloat16
F32 = jnp.float32
NZ = 16
NX = 4
NC = 2
NY = 4
CAP = 5
EXPERTS = NZ * NX
HK = NZ // NC
NQ = NX * NC
BLK = NQ * CAP
Z_ORDER = (0, 1, 7, 2, 6, 3, 5, 4)


def rdma(src, dst, send, recv, device):
    return pltpu.make_async_remote_copy(
        src_ref=src, dst_ref=dst, send_sem=send, recv_sem=recv, device_id=device, device_id_type=MESH
    )


def where_am_i():
    return tuple(lax.axis_index(a) for a in ("z", "x", "c", "y"))


def greet_all():
    z, x, c, y = where_am_i()
    barrier = pltpu.get_barrier_semaphore()

    def greet(device):
        pl.semaphore_signal(barrier, inc=1, device_id=device, device_id_type=MESH)

    for step in range(1, NQ):
        other = lax.rem(c * NX + x + step, NQ)
        greet((z, lax.rem(other, NX), other // NX, y))
    for step in range(1, NZ):
        greet((lax.rem(z + step, NZ), x, c, y))
    for step in range(1, NY):
        greet((z, x, c, lax.rem(y + step, NY)))


def wait_all():
    pl.semaphore_wait(pltpu.get_barrier_semaphore(), NQ - 1 + NZ - 1 + NY - 1)


def cols(index, width):
    return pl.ds(pl.multiple_of(index * width, width), width)


def permuted(perm_ref, value_ref, out_ref):
    width = value_ref.shape[-1]
    flat = value_ref[...].reshape(NQ * BLK, width)
    moved = jnp.dot(perm_ref[...], flat, preferred_element_type=F32).astype(BF)
    out_ref[...] = moved.reshape(NQ, BLK, width)


HALF = HK * BLK
LAG_F = 3
LAG_C = 6
PLAIN = (((1,), (0,)), ((), ()))
ROWS_BY = (((0,), (0,)), ((), ()))
COLS_BY = (((1,), (1,)), ((), ()))


def dot(a, b, dims):
    return lax.dot_general(a, b, dims, preferred_element_type=F32)


def gathered_rows(select_ref, value_ref):
    rows = dot(select_ref[...], value_ref[...], PLAIN).astype(BF)
    return rows.reshape(NQ, BLK, value_ref.shape[1])


def layer_kernel(
    sel_ref, selw_ref, tokens_ref, cot_ref, wt_ref, perm_ref, pick_ref, lane_ref,
    wg_hbm, wu_hbm, wd_hbm,
    out_ref, aux_out, moment_out, gain_out, full_ref, dense_ref, gate_out, up_out, down_out,
    *scratch,
):
    (
        s_tok, s_cot, x_tok, x_cot, p_tok, p_cot, rows_ref, grads_ref, wg, wu, wd, hid, dg, du,
        part, p_in, aux, aux_in, first, first_in, second_in, back, back_in, sorted_back, aux_sum,
        aux_y, aux_z, aux_t, moment_ref, m_in, m_half, m_x, m_xsum, m_z, g_mine, g_own, g_y,
        local_sem, x_send, x_recv, z_send, z_recv, yp_send, yp_recv, ym_send, ym_recv, f_send,
        f_recv, c_send, c_recv, g_send, g_recv, dz_send, dz_recv, dx_send, dx_recv, dc_send,
        dc_recv, mc_send, mc_recv, mx_send, mx_recv, mz_send, mz_recv, p_send, p_recv, b1_send,
        b1_recv, b2_send, b2_recv, ay_send, ay_recv, rz_send, rz_recv, rza_send, rza_recv, rx_send,
        rx_recv, rxa_send, rxa_recv, gy_send, gy_recv, gz_send, gz_recv, gx_send, gx_recv, gc_send,
        gc_recv,
    ) = scratch
    z, x, c, y = where_am_i()
    width = tokens_ref.shape[-1]
    me_q = c * NX + x
    y_up, y_down = lax.rem(y + 1, NY), lax.rem(y + NY - 1, NY)
    y_far = lax.rem(y + 2, NY)
    partner = (z, x, 1 - c, y)
    slots = (s_tok, s_cot)
    gathered = (x_tok, x_cot)
    sorted_rows = (p_tok, p_cot)
    outs = (rows_ref, grads_ref)

    own = [
        pltpu.make_async_copy(cot_ref, full_ref.at[:, cols(y, width)], local_sem.at[0]),
        pltpu.make_async_copy(wt_ref, dense_ref.at[z, x, c], local_sem.at[1]),
    ]
    for copy in own:
        copy.start()
    weights = [
        pltpu.make_async_copy(wg_hbm, wg, local_sem.at[6]),
        pltpu.make_async_copy(wu_hbm, wu, local_sem.at[7]),
        pltpu.make_async_copy(wd_hbm, wd, local_sem.at[8]),
    ]
    for copy in weights:
        copy.start()
    greet_all()
    slots[0][...] = gathered_rows(sel_ref, tokens_ref)
    slots[1][...] = gathered_rows(selw_ref, cot_ref)
    wait_all()

    def x_copy(a, step):
        other = lax.rem(me_q + step, NQ)
        return rdma(
            slots[a].at[other], gathered[a].at[me_q], x_send.at[a, step], x_recv.at[a, step],
            (z, lax.rem(other, NX), other // NX, y),
        )

    def x_arrival(a, step):
        source = lax.rem(me_q + NQ - step, NQ)
        return rdma(
            slots[a].at[source], gathered[a].at[source], x_send.at[a, step], x_recv.at[a, step],
            (z, lax.rem(source, NX), source // NX, y),
        )

    for a in range(2):
        for step in range(1, NQ):
            x_copy(a, step).start()

    def g_copy(step):
        return rdma(
            cot_ref, full_ref.at[:, cols(y, width)], g_send.at[step], g_recv.at[step],
            (z, x, c, lax.rem(y + step, NY)),
        )

    def g_arrival(step):
        source = lax.rem(y + NY - step, NY)
        return rdma(
            cot_ref, full_ref.at[:, cols(source, width)], g_send.at[step], g_recv.at[step],
            (z, x, c, source),
        )

    for step in range(1, NY):
        g_copy(step).start()

    def dz_copy(step):
        return rdma(
            wt_ref, dense_ref.at[z, x, c], dz_send.at[step], dz_recv.at[step],
            (lax.rem(z + step, NZ), x, c, y),
        )

    def dz_arrival(step):
        source = lax.rem(z + NZ - step, NZ)
        return rdma(
            wt_ref, dense_ref.at[source, x, c], dz_send.at[step], dz_recv.at[step], (source, x, c, y)
        )

    @pl.loop(1, NZ)
    def _(step):
        dz_copy(step).start()

    def z_copy(a, k):
        target = lax.rem(z + 2 * k + c, NZ)
        return rdma(
            sorted_rows[a].at[k], outs[a].at[c * HK + k, :, cols(y, width)],
            z_send.at[a, k], z_recv.at[a, k], (target, x, c, y),
        )

    def z_home(a):
        return pltpu.make_async_copy(
            sorted_rows[a].at[0], outs[a].at[0, :, cols(y, width)], local_sem.at[2 + a]
        )

    for a in range(2):
        gathered[a][me_q] = slots[a][me_q]
        for step in range(1, NQ):
            x_arrival(a, step).wait_recv()
        permuted(perm_ref, gathered[a], sorted_rows[a])
        for k in Z_ORDER:
            if k == 0:

                @pl.when(c == 0)
                def _():
                    z_home(a).start()

                @pl.when(c == 1)
                def _():
                    z_copy(a, 0).start()
            else:
                z_copy(a, k).start()

    def y_copy(a, k, up):
        part = outs[a].at[c * HK + k, :, cols(y, width)]
        if up:
            return rdma(part, part, yp_send.at[a, k], yp_recv.at[a, k], (z, x, c, y_up))
        return rdma(part, part, ym_send.at[a, k], ym_recv.at[a, k], (z, x, c, y_down))

    def y_arrival(a, k, up):
        if up:
            part = outs[a].at[c * HK + k, :, cols(y_down, width)]
            return rdma(part, part, yp_send.at[a, k], yp_recv.at[a, k], (z, x, c, y_down))
        part = outs[a].at[c * HK + k, :, cols(y_up, width)]
        return rdma(part, part, ym_send.at[a, k], ym_recv.at[a, k], (z, x, c, y_up))

    def f_copy(a, k):
        source, target = (y_down, y_up) if k % 2 == 0 else (y_up, y_down)
        part = outs[a].at[c * HK + k, :, cols(source, width)]
        return rdma(part, part, f_send.at[a, k], f_recv.at[a, k], (z, x, c, target))

    def f_arrival(a, k):
        part = outs[a].at[c * HK + k, :, cols(y_far, width)]
        return rdma(part, part, f_send.at[a, k], f_recv.at[a, k], (z, x, c, y_up))

    def c_copy(a, k):
        block = outs[a].at[c * HK + k]
        return rdma(block, block, c_send.at[a, k], c_recv.at[a, k], partner)

    def c_arrival(a, k):
        block = outs[a].at[(1 - c) * HK + k]
        return rdma(block, block, c_send.at[a, k], c_recv.at[a, k], partner)

    def dx_copy(step):
        part = dense_ref.at[:, x, c]
        return rdma(part, part, dx_send.at[step], dx_recv.at[step], (z, lax.rem(x + step, NX), c, y))

    def dx_arrival(step):
        source = lax.rem(x + NX - step, NX)
        part = dense_ref.at[:, source, c]
        return rdma(part, part, dx_send.at[step], dx_recv.at[step], (z, source, c, y))

    def dc_copy(core):
        part = dense_ref.at[:, :, core]
        return rdma(part, part, dc_send.at[0], dc_recv.at[0], partner)

    own[0].wait()
    for step in range(1, NY):
        g_arrival(step).wait_recv()
    moment_ref[...] = dot(full_ref[...], tokens_ref[...], ROWS_BY).reshape(moment_ref.shape)

    def mc_copy():
        return rdma(moment_ref.at[:, :, 1 - c], m_in, mc_send.at[0], mc_recv.at[0], partner)

    mc_copy().start()

    def mx_copy(step):
        other = lax.rem(x + step, NX)
        return rdma(m_half.at[:, other], m_x.at[step - 1], mx_send.at[step], mx_recv.at[step],
                    (z, other, c, y))

    def mz_copy(step):
        other = lax.rem(z + step, NZ)
        return rdma(m_xsum.at[other], m_z.at[step], mz_send.at[step], mz_recv.at[step],
                    (other, x, c, y))

    order = [(a, k) for a in range(2) for k in Z_ORDER]
    for i in range(len(order) + LAG_C):
        if i < len(order):
            a, k = order[i]
            if k == 0:

                @pl.when(c == 0)
                def _():
                    z_home(a).wait()

                @pl.when(c == 1)
                def _():
                    z_copy(a, 0).wait_recv()
            else:
                z_copy(a, k).wait_recv()
            y_copy(a, k, True).start()
            y_copy(a, k, False).start()
        if LAG_F <= i < len(order) + LAG_F:
            a, k = order[i - LAG_F]
            up = k % 2 == 0
            y_arrival(a, k, up).wait_recv()
            f_copy(a, k).start()
            y_arrival(a, k, not up).wait_recv()
        if i >= LAG_C:
            a, k = order[i - LAG_C]
            f_arrival(a, k).wait_recv()
            c_copy(a, k).start()
        if i == 6:
            own[1].wait()

            @pl.loop(1, NZ)
            def _(step):
                dz_arrival(step).wait_recv()

            for step in range(1, NX):
                dx_copy(step).start()
        if i == 8:
            mc_copy().wait_recv()
            for n in range(NX):
                m_half[:, n] = moment_ref[:, n, c] + m_in[:, n]
            for step in range(1, NX):
                mx_copy(step).start()
        if i == 12:
            for step in range(1, NX):
                dx_arrival(step).wait_recv()
            dc_copy(c).start()

    for step in range(1, NX):
        mx_copy(step).wait_recv()
    m_xsum[...] = m_half[:, x] + m_x[0] + m_x[1] + m_x[2]

    @pl.loop(1, NZ)
    def _(step):
        mz_copy(step).start()

    dc_copy(1 - c).wait_recv()
    for a, k in order:
        c_arrival(a, k).wait_recv()
    for copy in weights:
        copy.wait()

    def p_copy():
        return rdma(part.at[0], p_in, p_send.at[0], p_recv.at[0], partner)

    def pa_copy():
        return rdma(aux.at[0], aux_in, p_send.at[1], p_recv.at[1], partner)

    @pl.loop(0, 2)
    def _(turn):
        group = jnp.where(turn == 0, 1 - c, c)
        rows = rows_ref[pl.ds(group * HK, HK)].reshape(HALF, NY * width)
        grads = grads_ref[pl.ds(group * HK, HK)].reshape(HALF, NY * width)
        pre_gate = dot(rows, wg[...], PLAIN)
        pre_up = dot(rows, wu[...], PLAIN)
        back_h = dot(grads, wd[...], COLS_BY)
        sig = jax.nn.sigmoid(pre_gate)
        act = pre_gate * sig
        hidden_bf = (act * pre_up).astype(BF)
        hid[turn] = hidden_bf
        d_gate = (back_h * pre_up * sig * (1.0 + pre_gate * (1.0 - sig))).astype(BF)
        d_up = (back_h * act).astype(BF)
        dg[turn] = d_gate
        du[turn] = d_up
        route = jnp.sum(hidden_bf.astype(F32) * back_h, axis=1, keepdims=True)
        spread = route * lane_ref[...]
        high = spread.astype(BF)
        low = (spread - high.astype(F32)).astype(BF)
        placed = dot(pick_ref[...], high, PLAIN) + dot(pick_ref[...], low, PLAIN)
        aux[turn] = placed.reshape(HK, NQ, 128)
        both_parts = dot(d_gate, wg[...], COLS_BY) + dot(d_up, wu[...], COLS_BY)
        part[turn] = both_parts.astype(BF).reshape(HK, BLK, NY * width)

        @pl.when(turn == 0)
        def _():
            p_copy().start()
            pa_copy().start()

    half = HK // 2
    flip1 = y + 1 - 2 * lax.rem(y, 2)
    flip3 = NY - 1 - y
    flip2 = lax.rem(y + 2, NY)
    pairs = ((flip1, flip3), (flip3, flip1))

    p_copy().wait_recv()

    def b1_copy(h):
        return rdma(
            first.at[h, pl.ds(2, 2)], first_in.at[h], b1_send.at[h], b1_recv.at[h],
            (z, x, c, pairs[h][0]),
        )

    def both(h, i, owner):
        for j in range(half):
            mine = part[1, h * half + j, :, cols(owner, width)].astype(F32)
            theirs = p_in[h * half + j, :, cols(owner, width)].astype(F32)
            first[h, i, j] = (mine + theirs).astype(BF)

    for h in range(2):
        both(h, 2, pairs[h][0])
        both(h, 3, flip2)
        b1_copy(h).start()
    for h in range(2):
        both(h, 0, y)
        both(h, 1, pairs[h][1])

    pa_copy().wait_recv()
    aux_sum[...] = aux[1] + aux_in[...]

    def ay_copy(step):
        return rdma(aux_sum, aux_y.at[y], ay_send.at[step], ay_recv.at[step],
                    (z, x, c, lax.rem(y + step, NY)))

    def ay_arrival(step):
        source = lax.rem(y + NY - step, NY)
        return rdma(aux_sum, aux_y.at[source], ay_send.at[step], ay_recv.at[step], (z, x, c, source))

    for step in range(1, NY):
        ay_copy(step).start()
    aux_y[y] = aux_sum[...]

    def b2_copy(h):
        return rdma(first.at[h, 3], second_in.at[h], b2_send.at[h], b2_recv.at[h],
                    (z, x, c, pairs[h][1]))

    for h in range(2):
        b1_copy(h).wait()
        first[h, 3] = (first[h, 1].astype(F32) + first_in[h, 1].astype(F32)).astype(BF)
        b2_copy(h).start()

    m_z[0] = m_xsum[z]

    @pl.loop(1, NZ)
    def _(step):
        mz_copy(step).wait()

    moment_own = jnp.sum(m_z[...], axis=0)
    moment_out[...] = moment_own
    gain = jnp.sum(wt_ref[...].astype(F32) * moment_own, axis=1, keepdims=True)
    g_mine[...] = jnp.broadcast_to(gain, g_mine.shape)

    def gy_copy(step):
        return rdma(g_mine, g_y.at[y], gy_send.at[step], gy_recv.at[step],
                    (z, x, c, lax.rem(y + step, NY)))

    def gy_arrival(step):
        source = lax.rem(y + NY - step, NY)
        return rdma(g_mine, g_y.at[source], gy_send.at[step], gy_recv.at[step], (z, x, c, source))

    for step in range(1, NY):
        gy_copy(step).start()
    g_y[y] = g_mine[...]

    for step in range(1, NY):
        ay_arrival(step).wait_recv()
        ay_copy(step).wait_send()
    aux_sum[...] = aux_y[0] + aux_y[1] + aux_y[2] + aux_y[3]

    def r_z_copy(k):
        target = lax.rem(z + 2 * NZ - 2 * k - c, NZ)
        return rdma(back.at[k], back_in.at[k], rz_send.at[k], rz_recv.at[k], (target, x, c, y))

    def r_za_copy(k):
        target = lax.rem(z + 2 * NZ - 2 * k - c, NZ)
        return rdma(aux_sum.at[k], aux_z.at[k], rza_send.at[k], rza_recv.at[k], (target, x, c, y))

    r_z_home = [
        pltpu.make_async_copy(back.at[0], back_in.at[0], local_sem.at[4]),
        pltpu.make_async_copy(aux_sum.at[0], aux_z.at[0], local_sem.at[5]),
    ]

    def send_back(k):
        if k == 0:

            @pl.when(c == 0)
            def _():
                r_z_home[0].start()
                r_z_home[1].start()

            @pl.when(c == 1)
            def _():
                r_z_copy(0).start()
                r_za_copy(0).start()
        else:
            r_z_copy(k).start()
            r_za_copy(k).start()

    for h in range(2):
        b2_copy(h).wait()
        back[pl.ds(h * half, half)] = (
            first[h, 0].astype(F32) + first_in[h, 0].astype(F32) + second_in[h].astype(F32)
        ).astype(BF)
    for k in reversed(Z_ORDER):
        send_back(k)

    for step in range(1, NY):
        gy_arrival(step).wait_recv()
    g_own[...] = g_y[0] + g_y[1] + g_y[2] + g_y[3]

    def gz_copy(step):
        return rdma(g_own, gain_out.at[z, x, c], gz_send.at[step], gz_recv.at[step],
                    (lax.rem(z + step, NZ), x, c, y))

    def gz_arrival(step):
        source = lax.rem(z + NZ - step, NZ)
        return rdma(g_own, gain_out.at[source, x, c], gz_send.at[step], gz_recv.at[step],
                    (source, x, c, y))

    @pl.loop(1, NZ)
    def _(step):
        gz_copy(step).start()

    gain_out[z, x, c] = g_own[...]

    def over_rows(a, b):
        return dot(a, b, ROWS_BY)

    grows = (rows_ref[pl.ds((1 - c) * HK, HK)].reshape(HALF, NY * width), rows_ref[pl.ds(c * HK, HK)].reshape(HALF, NY * width))
    ggrads = (grads_ref[pl.ds((1 - c) * HK, HK)].reshape(HALF, NY * width), grads_ref[pl.ds(c * HK, HK)].reshape(HALF, NY * width))
    gate_out[...] = (over_rows(grows[0], dg[0]) + over_rows(grows[1], dg[1])).astype(BF)
    up_out[...] = (over_rows(grows[0], du[0]) + over_rows(grows[1], du[1])).astype(BF)
    down_out[...] = (over_rows(hid[0], ggrads[0]) + over_rows(hid[1], ggrads[1])).astype(BF)

    @pl.loop(1, NZ)
    def _(step):
        gz_arrival(step).wait_recv()

    def gx_copy(step):
        tiles = gain_out.at[:, x, c]
        return rdma(tiles, tiles, gx_send.at[step], gx_recv.at[step], (z, lax.rem(x + step, NX), c, y))

    def gx_arrival(step):
        source = lax.rem(x + NX - step, NX)
        tiles = gain_out.at[:, source, c]
        return rdma(tiles, tiles, gx_send.at[step], gx_recv.at[step], (z, source, c, y))

    for step in range(1, NX):
        gx_copy(step).start()

    def gc_copy(core):
        tiles = gain_out.at[:, :, core]
        return rdma(tiles, tiles, gc_send.at[0], gc_recv.at[0], partner)

    for k in Z_ORDER:
        if k == 0:

            @pl.when(c == 0)
            def _():
                r_z_home[0].wait()
                r_z_home[1].wait()

            @pl.when(c == 1)
            def _():
                r_z_copy(0).wait()
                r_za_copy(0).wait()
        else:
            r_z_copy(k).wait()
            r_za_copy(k).wait()
    permuted(perm_ref, back_in, sorted_back)
    for q in range(NQ):
        aux_t[q] = aux_z[:, q, :]

    def r_x_copy(step):
        other = lax.rem(me_q + step, NQ)
        return rdma(sorted_back.at[other], out_ref.at[me_q], rx_send.at[step], rx_recv.at[step],
                    (z, lax.rem(other, NX), other // NX, y))

    def r_xa_copy(step):
        other = lax.rem(me_q + step, NQ)
        return rdma(aux_t.at[other], aux_out.at[me_q], rxa_send.at[step], rxa_recv.at[step],
                    (z, lax.rem(other, NX), other // NX, y))

    def r_x_arrival(step):
        source = lax.rem(me_q + NQ - step, NQ)
        device = (z, lax.rem(source, NX), source // NX, y)
        return (
            rdma(sorted_back.at[source], out_ref.at[source], rx_send.at[step], rx_recv.at[step], device),
            rdma(aux_t.at[source], aux_out.at[source], rxa_send.at[step], rxa_recv.at[step], device),
        )

    for step in range(1, NQ):
        r_x_copy(step).start()
        r_xa_copy(step).start()
    out_ref[me_q] = sorted_back[me_q]
    aux_out[me_q] = aux_t[me_q]

    for step in range(1, NX):
        gx_arrival(step).wait_recv()
    gc_copy(c).start()
    gc_copy(1 - c).wait_recv()
    for step in range(1, NQ):
        for arrival in r_x_arrival(step):
            arrival.wait_recv()
    for step in range(1, NQ):
        r_x_copy(step).wait_send()
        r_xa_copy(step).wait_send()
    p_copy().wait_send()
    pa_copy().wait_send()
    gc_copy(c).wait_send()
    for step in range(1, NX):
        gx_copy(step).wait_send()
    for step in range(1, NY):
        gy_copy(step).wait_send()

    @pl.loop(1, NZ)
    def _(step):
        gz_copy(step).wait_send()

    for a in range(2):
        for step in range(1, NQ):
            x_copy(a, step).wait_send()
    for step in range(1, NY):
        g_copy(step).wait_send()

    @pl.loop(1, NZ)
    def _(step):
        dz_copy(step).wait_send()

    for step in range(1, NX):
        dx_copy(step).wait_send()
    dc_copy(c).wait_send()
    for a, k in order:
        if k == 0:

            @pl.when(c == 1)
            def _():
                z_copy(a, 0).wait_send()
        else:
            z_copy(a, k).wait_send()
        y_copy(a, k, True).wait_send()
        y_copy(a, k, False).wait_send()
        f_copy(a, k).wait_send()
        c_copy(a, k).wait_send()
    mc_copy().wait_send()
    for step in range(1, NX):
        mx_copy(step).wait_send()


VMEM_SPEC = pl.BlockSpec(memory_space=pltpu.VMEM)
HBM_SPEC = pl.BlockSpec(memory_space=pl.ANY)
DMA = pltpu.SemaphoreType.DMA


def layer(select, select_weighted, tokens, cotangent, wt, perm, pick, lane, gate, up, down):
    width = tokens.shape[1]
    half = HK // 2
    own = wt.shape[0]
    vm = pltpu.VMEM
    shape = jax.ShapeDtypeStruct
    return pl.pallas_call(
        layer_kernel,
        out_shape=(
            shape((NQ, BLK, width), BF),
            shape((NQ, HK, 128), F32),
            shape((own, width), F32),
            shape((NZ, NX, NC, own, 128), F32),
            shape((tokens.shape[0], NY * width), BF),
            shape((NZ, NX, NC) + wt.shape, BF),
            shape(gate.shape, BF),
            shape(up.shape, BF),
            shape(down.shape, BF),
        ),
        in_specs=[VMEM_SPEC] * 8 + [HBM_SPEC] * 3,
        out_specs=(VMEM_SPEC,) * 9,
        scratch_shapes=[
            vm((NQ, BLK, width), BF),
            vm((NQ, BLK, width), BF),
            vm((NQ, BLK, width), BF),
            vm((NQ, BLK, width), BF),
            vm((NQ, BLK, width), BF),
            vm((NQ, BLK, width), BF),
            vm((NZ, BLK, NY * width), BF),
            vm((NZ, BLK, NY * width), BF),
            vm(gate.shape, BF),
            vm(gate.shape, BF),
            vm(down.shape, BF),
            vm((2, HALF, gate.shape[1]), BF),
            vm((2, HALF, gate.shape[1]), BF),
            vm((2, HALF, gate.shape[1]), BF),
            vm((2, HK, BLK, NY * width), BF),
            vm((HK, BLK, NY * width), BF),
            vm((2, HK, NQ, 128), F32),
            vm((HK, NQ, 128), F32),
            vm((2, NY, half, BLK, width), BF),
            vm((2, 2, half, BLK, width), BF),
            vm((2, half, BLK, width), BF),
            vm((HK, BLK, width), BF),
            vm((HK, BLK, width), BF),
            vm((NQ, BLK, width), BF),
            vm((HK, NQ, 128), F32),
            vm((NY, HK, NQ, 128), F32),
            vm((HK, NQ, 128), F32),
            vm((NQ, HK, 128), F32),
            vm((NZ, NX, NC, own, width), F32),
            vm((NZ, NX, own, width), F32),
            vm((NZ, NX, own, width), F32),
            vm((NX - 1, NZ, own, width), F32),
            vm((NZ, own, width), F32),
            vm((NZ, own, width), F32),
            vm((own, 128), F32),
            vm((own, 128), F32),
            vm((NY, own, 128), F32),
            DMA((9,)),
            DMA((2, NQ)),
            DMA((2, NQ)),
            DMA((2, HK)),
            DMA((2, HK)),
            DMA((2, HK)),
            DMA((2, HK)),
            DMA((2, HK)),
            DMA((2, HK)),
            DMA((2, HK)),
            DMA((2, HK)),
            DMA((2, HK)),
            DMA((2, HK)),
            DMA((NY,)),
            DMA((NY,)),
            DMA((NZ,)),
            DMA((NZ,)),
            DMA((NX,)),
            DMA((NX,)),
            DMA((1,)),
            DMA((1,)),
            DMA((1,)),
            DMA((1,)),
            DMA((NX,)),
            DMA((NX,)),
            DMA((NZ,)),
            DMA((NZ,)),
            DMA((2,)),
            DMA((2,)),
            DMA((2,)),
            DMA((2,)),
            DMA((2,)),
            DMA((2,)),
            DMA((NY,)),
            DMA((NY,)),
            DMA((HK,)),
            DMA((HK,)),
            DMA((HK,)),
            DMA((HK,)),
            DMA((NQ,)),
            DMA((NQ,)),
            DMA((NQ,)),
            DMA((NQ,)),
            DMA((NY,)),
            DMA((NY,)),
            DMA((NZ,)),
            DMA((NZ,)),
            DMA((NX,)),
            DMA((NX,)),
            DMA((1,)),
            DMA((1,)),
        ],
        compiler_params=pltpu.CompilerParams(
            collective_id=0, has_side_effects=True, vmem_limit_bytes=60 * 1024 * 1024
        ),
        name="layer",
    )(select, select_weighted, tokens, cotangent, wt, perm, pick, lane, gate, up, down)


def local(tokens, cotangent, routes, route_weights, w_gate, w_up, w_down, dense_weight, mix_gate):
    z, x, c = (lax.axis_index(a) for a in EP)
    token_count = routes.shape[0]
    ep_count = NZ * NX * NC
    e = jnp.arange(EXPERTS, dtype=jnp.int32)
    expert = lax.rem(z + 2 * lax.rem(e, HK) + e // (HK * NX), NZ) * NX + lax.rem(e // HK, NX)
    picked = routes.T
    hits = [picked[p][None, :] == expert[:, None] for p in range(2)]
    hit = hits[0] | hits[1]
    t = jnp.arange(token_count, dtype=jnp.int32)
    earlier = (t[:, None] < t[None, :]).astype(BF)
    rank = jnp.dot(hit.astype(BF), earlier, preferred_element_type=F32).astype(jnp.int32)
    s = jnp.arange(CAP, dtype=jnp.int32)
    chosen = (hit[:, None, :] & (rank[:, None, :] == s[None, :, None])).reshape(-1, token_count)
    weights = route_weights.T
    weight = jnp.where(hits[0], weights[0][None, :], weights[1][None, :])
    weight = jnp.broadcast_to(weight[:, None, :], (EXPERTS, CAP, token_count)).reshape(-1, token_count)
    select = chosen.astype(BF)
    select_weighted = jnp.where(chosen, weight, jnp.zeros_like(weight))
    r = jnp.arange(NQ * BLK, dtype=jnp.int32)
    moved = lax.rem(r, BLK) // CAP * BLK + r // BLK * CAP + lax.rem(r, CAP)
    perm = (moved[:, None] == r[None, :]).astype(BF)
    groups = jnp.arange(HK * NQ, dtype=jnp.int32)
    pick = (r[None, :] // CAP == groups[:, None]).astype(BF)
    lane = (lax.rem(r, CAP)[:, None] == jnp.arange(128, dtype=jnp.int32)[None, :]).astype(F32)
    slots, aux_back, moment_own, gain_all, cot_full, wt_full, gate_grad, up_grad, down_grad = layer(
        select, select_weighted, tokens, cotangent, dense_weight.T, perm, pick, lane,
        w_gate[0], w_up[0], w_down[0],
    )
    own = dense_weight.shape[1]
    wt_full = wt_full.reshape(ep_count * own, -1)
    scaled = (mix_gate[None, :] * cot_full.astype(F32)).astype(BF)
    dense_dx = jnp.dot(scaled, wt_full, preferred_element_type=F32)
    token_grad = (dense_dx + dot(select, slots.reshape(NQ * BLK, -1), ROWS_BY)).astype(BF)
    values = aux_back[:, :, :CAP].reshape(EXPERTS, CAP)
    at_slot = jnp.sum(
        jnp.where(rank[:, :, None] == s[None, None, :], values[:, None, :], 0.0), axis=2
    )
    route_sums = jnp.stack([jnp.sum(jnp.where(h, at_slot, 0.0), axis=0) for h in hits], axis=1)
    route_grad = route_sums / route_weights.astype(F32)
    ep_index = (z * NX + x) * NC + c
    own_gate = lax.dynamic_slice(mix_gate, (ep_index * own,), (own,))
    dense_grad = (moment_own * (own_gate[:, None] * (1.0 / ep_count))).T
    mix_grad = gain_all[..., 0].reshape(-1) / ep_count
    return token_grad, route_grad, gate_grad[None], up_grad[None], down_grad[None], dense_grad, mix_grad


def solution(mesh):
    finer = Mesh(mesh.devices.reshape(NZ, NX, NC, NY), EP + ("y",))
    in_specs = (
        P(EP, "y"),
        P(EP, "y"),
        P(EP, None),
        P(EP, None),
        P(EP, None, "y"),
        P(EP, None, "y"),
        P(EP, "y", None),
        P("y", EP),
        P(),
    )
    out_specs = (
        P(EP, "y"),
        P(EP, None),
        P(EP, None, "y"),
        P(EP, None, "y"),
        P(EP, "y", None),
        P("y", EP),
        P(),
    )
    return jax.shard_map(local, mesh=finer, in_specs=in_specs, out_specs=out_specs, check_vma=False)
```

time: 137 us -> 115 us (0.84)
  Pallas kernels: 111 us -> 96 us
  matrix products: 17.5 us -> 3.25 us
  local copies, waits for them, and re-layouts: 4.3 us -> 8.59 us
  other arithmetic: 3.29 us -> 5.68 us
    pallas_call x2 -> x1, Pallas kernels: 111 us -> 96 us  [layer(): pl.pallas_call(layer_kernel, out_shape=(shape((NQ, BLK, width), BF), shap...]
    dot_general x8 -> x1, matrix products: 11.7 us -> 1.23 us  [dot(): return lax.dot_general(a, b, dims, preferred_element_type=F32)]
    unnamed x26 -> x27, local copies, waits for them, and re-layouts: 0.75 us -> 6.58 us
    dot_general x4 -> x0, matrix products: 4.68 us -> none  [the longest x1 2.18 us: local(): pre_up = jnp.dot(rows_in, up_matrix, preferred_element_type=F32)]
    convert_element_type x0 -> x3, other arithmetic: none -> 2.06 us  [the longest x1 0.78 us: local(): (lax.rem(r, CAP)[:, None] == jnp.arange(128, dtype=jnp.int32)[None, :]).a...]
where the time goes in v2:
time: 115 us; the launch traced here: 114 us
  Pallas kernels  96 us (83%)
  local copies, waits for them, and re-layouts  8.59 us (7%)
  other arithmetic  5.68 us (5%)
  matrix products  3.25 us (3%)
    pallas_call x1, Pallas kernels, layer(): pl.pallas_call(layer_kernel, out_shape=(shape((NQ, BLK, width), BF), shap...  96 us
    unnamed x27, local copies, waits for them, and re-layouts  6.58 us

profile of v2, /device:TPU:1, one launch (start us, length us, event | category | flops | bytes accessed | tf_op | source)
XLA Modules:
  0.0 114.3 jit_solution(6576463104407732650)
XLA Ops:
  0.7 0.0 copy-start.10
  0.7 0.7 copy-done.10
  1.3 0.2 convolution_convert_fusion
  1.5 0.0 copy-start.8
  1.6 0.0 copy-start.2
  1.6 0.1 compare_or_fusion
  1.8 0.4 copy-done.8
  2.2 0.1 compare_select_fusion.1
  2.4 0.1 eq.132
  2.5 0.8 broadcast_select_fusion
  3.3 0.6 convert_element_type.30.sel_ref
  3.9 0.0 copy-done.2
  3.9 0.0 copy-start.3
  3.9 1.2 %copy.24 = bf16[1,1024,352]{2,1,0:T(8,128)(2,1)} copy(bf16[1,1024,352]{1,2,0:T(8,128)(2,1)S(1)} %copy-done.2) | data formatting | bytes 1441792 | tf_op args[4]
  5.1 0.0 copy-done.3
  5.1 1.2 %copy.25 = bf16[1,1024,352]{2,1,0:T(8,128)(2,1)} copy(bf16[1,1024,352]{1,2,0:T(8,128)(2,1)S(1)} %copy-done.3) | data formatting | bytes 1441792 | tf_op args[5]
  6.3 0.8 fusion.1.perm_ref
  7.1 0.8 fusion.4.lane_ref
  7.9 0.6 fusion.5.pick_ref
  8.5 96.0 %layer.1 = (bf16[8,40,256]{2,1,0:T(8,128)(2,1)}, f32[8,8,128]{2,1,0:T(8,128)}, f32[8,256]{1,0:T(8,128)}, f32[16,4,2,8,128]{4,3,2,1,0:T(8,128)}, bf16[128,1024]{1...) custom-call(bf16[320,128]{1,0:T(8,128)(2,1)} %convert_element_type.3, ...), custom_call_target="tpu_custom_call" | custom-call | tf_op jit(solution)/shard_map/layer/pallas_call | solution.py:640
  104.5 0.0 copy-start.6
  104.5 0.8 slice_bitcast_fusion
  105.3 0.1 copy.26
  105.4 0.0 copy-start.9
  105.4 0.1 select_reduce_fusion
  105.5 0.1 fusion.7
  105.6 0.6 maximum_divide_fusion
  106.2 0.0 copy-start.1
  106.2 0.1 fusion.3
  106.3 1.2 %fusion.26 = f32[128,256]{1,0:T(8,128)S(1)} fusion(pred[320,128]{1,0:T(32,128)(4,1)S(1)} %and.93, bf16[320,256]{1,0:T(8,128)(2,1)} %bitcast.35), kind=kOutput, calls=%fused_computation.67 | convolution fusion | flops 20971520 | bytes 335872 | tf_op jit(solution)/shard_map/dot_general | solution.py:75
  107.6 0.0 copy-done.6
  107.6 0.0 copy-done.9
  107.6 0.0 copy-start.7
  107.6 1.8 %fusion = bf16[128,256]{1,0:T(8,128)(2,1)} fusion(f32[128,256]{1,0:T(8,128)S(1)} %fusion.26, bf16[1024,256]{1,0:T(8,128)(2,1)S(1)} %bitcast.34, bf16[128,1024]{1,0:T(8,128)(2,1)} %get-tuple-element.16, f32[1024]{0:T(1024)S(1)} %copy-done.9), kind=kOutput, calls=%fused_computation.1 | convolution fusion | flops 67567616 | bytes 987136 | tf_op jit(solution)/shard_map/dot_general | solution.py:784
  109.4 0.0 copy-start
  109.4 0.1 dynamic-slice_multiply_fusion
  109.5 0.0 copy-done.7
  109.5 0.7 multiply_bitcast_fusion
  110.2 0.0 copy-done.1
  110.2 1.1 copy.27
  111.3 0.0 copy-done
  111.3 0.0 copy-start.5
  111.3 1.1 copy.28
  112.5 0.0 copy-done.5
  112.5 0.3 multiply_reduce_fusion
  112.7 0.7 div.64
  113.5 0.0 copy-done.4
  113.5 0.9 copy.31
  (15 shorter events, 0.3 us)
Async XLA Ops:
  0.7 0.7 copy-start.10
  1.5 0.7 copy-start.8
  1.6 2.3 %copy-start.2 = (bf16[1,1024,352]{1,2,0:T(8,128)(2,1)S(1)}, bf16[1,1024,352]{1,2,0:T(8,128)(2,1)}, u32[]{:S(2)}) copy-start(bf16[1,1024,352]{1,2,0:T(8,128)(2,1)} %param.13) | copy-start | bytes 2162692
  3.9 1.2 %copy-start.3 = (bf16[1,1024,352]{1,2,0:T(8,128)(2,1)S(1)}, bf16[1,1024,352]{1,2,0:T(8,128)(2,1)}, u32[]{:S(2)}) copy-start(bf16[1,1024,352]{1,2,0:T(8,128)(2,1)} %param.14) | copy-start | bytes 2162692
  104.5 3.1 %copy-start.6 = (bf16[16,4,2,8,256]{4,3,2,1,0:T(8,128)(2,1)S(1)}, bf16[16,4,2,8,256]{4,3,2,1,0:T(8,128)(2,1)}, u32[]{:S(2)}) copy-start(bf16[16,4,2,8,256]{4,3,2,1,0:T(8,128)(2,1)} %get-tuple-element.17) | copy-start | bytes 1572868
  105.4 2.2 %copy-start.9 = (f32[1024]{0:T(1024)S(1)}, f32[1024]{0:T(1024)}, u32[]{:S(2)}) copy-start(f32[1024]{0:T(1024)} %param.17) | copy-start | bytes 12292
  106.2 4.0 %copy-start.1 = (bf16[1024,352]{1,0:T(8,128)(2,1)S(1)}, bf16[1024,352]{1,0:T(8,128)(2,1)}, u32[]{:S(2)}) copy-start(bf16[1024,352]{1,0:T(8,128)(2,1)} %get-tuple-element.20) | copy-start | bytes 2162692
  107.6 1.9 %copy-start.7 = (f32[8,256]{1,0:T(8,128)S(1)}, f32[8,256]{1,0:T(8,128)}, u32[]{:S(2)}) copy-start(f32[8,256]{1,0:T(8,128)} %get-tuple-element.23) | copy-start | bytes 24580
  109.4 1.9 %copy-start = (bf16[1024,352]{1,0:T(8,128)(2,1)S(1)}, bf16[1024,352]{1,0:T(8,128)(2,1)}, u32[]{:S(2)}) copy-start(bf16[1024,352]{1,0:T(8,128)(2,1)} %get-tuple-element.21) | copy-start | bytes 2162692
  111.3 1.1 %copy-start.5 = (f32[16,4,2,8,128]{4,3,2,1,0:T(8,128)S(1)}, f32[16,4,2,8,128]{4,3,2,1,0:T(8,128)}, u32[]{:S(2)}) copy-start(f32[16,4,2,8,128]{4,3,2,1,0:T(8,128)} %get-tuple-element.24) | copy-start | bytes 1572868
  111.3 2.1 %copy-start.4 = (bf16[352,1024]{1,0:T(8,128)(2,1)S(1)}, bf16[352,1024]{1,0:T(8,128)(2,1)}, u32[]{:S(2)}) copy-start(bf16[352,1024]{1,0:T(8,128)(2,1)} %get-tuple-element.22) | copy-start | bytes 2162692

commit v3 on v2

--- a/solution.py
+++ b/solution.py
@@ -1,3 +1,5 @@
+import functools
+
 import jax
 import jax.numpy as jnp
 from jax import lax
@@ -15,7 +17,6 @@
 NC = 2
 NY = 4
 CAP = 5
-EXPERTS = NZ * NX
 HK = NZ // NC
 NQ = NX * NC
 BLK = NQ * CAP
@@ -75,15 +76,37 @@
     return lax.dot_general(a, b, dims, preferred_element_type=F32)
 
 
-def gathered_rows(select_ref, value_ref):
-    rows = dot(select_ref[...], value_ref[...], PLAIN).astype(BF)
+def gathered_rows(select, value_ref):
+    rows = dot(select, value_ref[...], PLAIN).astype(BF)
     return rows.reshape(NQ, BLK, value_ref.shape[1])
 
 
+def over_40(value):
+    return (value * 52429) >> 21
+
+
+def over_5(value):
+    return (value * 52429) >> 18
+
+
+def iota(shape, dim):
+    return lax.broadcasted_iota(jnp.int32, shape, dim)
+
+
+def ones_where(mask, dtype):
+    return jnp.where(mask, 1.0, 0.0).astype(dtype)
+
+
+def exact_dot(one_hot, value):
+    high = value.astype(BF)
+    low = (value - high.astype(F32)).astype(BF)
+    return dot(one_hot, high, PLAIN) + dot(one_hot, low, PLAIN)
+
+
 def layer_kernel(
-    sel_ref, selw_ref, tokens_ref, cot_ref, wt_ref, perm_ref, pick_ref, lane_ref,
+    tokens_ref, cot_ref, routes_ref, weights_ref, wt_ref, mix_ref,
     wg_hbm, wu_hbm, wd_hbm,
-    out_ref, aux_out, moment_out, gain_out, full_ref, dense_ref, gate_out, up_out, down_out,
+    token_out, route_out, gate_out, up_out, down_out, dense_out, mix_out,
     *scratch,
 ):
     (
@@ -96,6 +119,8 @@
         b1_recv, b2_send, b2_recv, ay_send, ay_recv, rz_send, rz_recv, rza_send, rza_recv, rx_send,
         rx_recv, rxa_send, rxa_recv, gy_send, gy_recv, gz_send, gz_recv, gx_send, gx_recv, gc_send,
         gc_recv,
+        perm_ref, sel_ref, chosen_ref, full_ref, dense_ref, out_ref, aux_out, az_out, gain_out, pg, pu, dx_acc,
+        gate_s, up_s, down_s, put_sem,
     ) = scratch
     z, x, c, y = where_am_i()
     width = tokens_ref.shape[-1]
@@ -122,8 +147,36 @@
     for copy in weights:
         copy.start()
     greet_all()
-    slots[0][...] = gathered_rows(sel_ref, tokens_ref)
-    slots[1][...] = gathered_rows(selw_ref, cot_ref)
+    table = (NQ * BLK, tokens_ref.shape[0])
+    row = iota(table, 0)
+    line = over_40(row)
+    rest = row - BLK * line
+    step_k = over_5(rest)
+    slot = rest - CAP * step_k
+    expert = ((z + 2 * step_k + (line >> 2)) & (NZ - 1)) * NX + (line & (NX - 1))
+    hit_first = routes_ref[0:1, :] == expert
+    hit_second = routes_ref[1:2, :] == expert
+    square = (table[1], table[1])
+    earlier = ones_where(iota(square, 0) < iota(square, 1), BF)
+    hit = ones_where(hit_first, F32) + ones_where(hit_second, F32)
+    rank = dot(hit.astype(BF), earlier, PLAIN)
+    at_slot = ones_where(rank == slot.astype(F32), F32)
+    chosen_ref[0] = ones_where(hit_first, F32) * at_slot
+    chosen_ref[1] = ones_where(hit_second, F32) * at_slot
+    gate_weights = weights_ref[...].astype(F32)
+    select = (hit * at_slot).astype(BF)
+    sel_ref[...] = select
+    select_weighted = (chosen_ref[0] * gate_weights[0:1, :] + chosen_ref[1] * gate_weights[1:2, :]).astype(BF)
+    slots[0][...] = gathered_rows(select, tokens_ref)
+    slots[1][...] = gathered_rows(select_weighted, cot_ref)
+    both_ways = (NQ * BLK, NQ * BLK)
+    place = iota(both_ways, 0)
+    block = over_40(place)
+    inside = place - BLK * block
+    source = over_5(inside)
+    perm_ref[...] = ones_where(
+        source * BLK + block * CAP + (inside - CAP * source) == iota(both_ways, 1), BF
+    )
     wait_all()
 
     def x_copy(a, step):
@@ -268,6 +321,10 @@
         other = lax.rem(z + step, NZ)
         return rdma(m_xsum.at[other], m_z.at[step], mz_send.at[step], mz_recv.at[step],
                     (other, x, c, y))
+
+    def rows_of(ref, turn):
+        group = jnp.where(turn == 0, 1 - c, c)
+        return ref[pl.ds(group * HK, HK)].reshape(HALF, NY * width)
 
     order = [(a, k) for a in range(2) for k in Z_ORDER]
     for i in range(len(order) + LAG_C):
@@ -311,24 +368,33 @@
                 m_half[:, n] = moment_ref[:, n, c] + m_in[:, n]
             for step in range(1, NX):
                 mx_copy(step).start()
+        if i == 13:
+            for copy in weights:
+                copy.wait()
+            for k in Z_ORDER:
+                c_arrival(0, k).wait_recv()
+        if 14 <= i < 18:
+            turn = (i - 14) // 2
+            if i % 2 == 0:
+                pg[turn] = dot(rows_of(rows_ref, turn), wg[...], COLS_BY)
+            else:
+                pu[turn] = dot(rows_of(rows_ref, turn), wu[...], COLS_BY)
+        if i == 20:
+            for step in range(1, NX):
+                mx_copy(step).wait_recv()
+            m_xsum[...] = m_half[:, x] + m_x[0] + m_x[1] + m_x[2]
+
+            @pl.loop(1, NZ)
+            def _(step):
+                mz_copy(step).start()
         if i == 12:
             for step in range(1, NX):
                 dx_arrival(step).wait_recv()
             dc_copy(c).start()
 
-    for step in range(1, NX):
-        mx_copy(step).wait_recv()
-    m_xsum[...] = m_half[:, x] + m_x[0] + m_x[1] + m_x[2]
-
-    @pl.loop(1, NZ)
-    def _(step):
-        mz_copy(step).start()
-
     dc_copy(1 - c).wait_recv()
-    for a, k in order:
-        c_arrival(a, k).wait_recv()
-    for copy in weights:
-        copy.wait()
+    for k in Z_ORDER:
+        c_arrival(1, k).wait_recv()
 
     def p_copy():
         return rdma(part.at[0], p_in, p_send.at[0], p_recv.at[0], partner)
@@ -338,12 +404,9 @@
 
     @pl.loop(0, 2)
     def _(turn):
-        group = jnp.where(turn == 0, 1 - c, c)
-        rows = rows_ref[pl.ds(group * HK, HK)].reshape(HALF, NY * width)
-        grads = grads_ref[pl.ds(group * HK, HK)].reshape(HALF, NY * width)
-        pre_gate = dot(rows, wg[...], PLAIN)
-        pre_up = dot(rows, wu[...], PLAIN)
-        back_h = dot(grads, wd[...], COLS_BY)
+        pre_gate = pg[turn]
+        pre_up = pu[turn]
+        back_h = dot(rows_of(grads_ref, turn), wd[...], COLS_BY)
         sig = jax.nn.sigmoid(pre_gate)
         act = pre_gate * sig
         hidden_bf = (act * pre_up).astype(BF)
@@ -353,12 +416,11 @@
         dg[turn] = d_gate
         du[turn] = d_up
         route = jnp.sum(hidden_bf.astype(F32) * back_h, axis=1, keepdims=True)
-        spread = route * lane_ref[...]
-        high = spread.astype(BF)
-        low = (spread - high.astype(F32)).astype(BF)
-        placed = dot(pick_ref[...], high, PLAIN) + dot(pick_ref[...], low, PLAIN)
-        aux[turn] = placed.reshape(HK, NQ, 128)
-        both_parts = dot(d_gate, wg[...], COLS_BY) + dot(d_up, wu[...], COLS_BY)
+        at = (HALF, 128)
+        lane_is = over_40(iota(at, 0)) * -BLK + iota(at, 0) == iota(at, 1)
+        block_of = ones_where(over_40(iota((HK, HALF), 1)) == iota((HK, HALF), 0), BF)
+        aux[turn] = exact_dot(block_of, jnp.where(lane_is, route, 0.0))
+        both_parts = dot(d_gate, wg[...], PLAIN) + dot(d_up, wu[...], PLAIN)
         part[turn] = both_parts.astype(BF).reshape(HK, BLK, NY * width)
 
         @pl.when(turn == 0)
@@ -418,33 +480,12 @@
         first[h, 3] = (first[h, 1].astype(F32) + first_in[h, 1].astype(F32)).astype(BF)
         b2_copy(h).start()
 
-    m_z[0] = m_xsum[z]
-
-    @pl.loop(1, NZ)
-    def _(step):
-        mz_copy(step).wait()
-
-    moment_own = jnp.sum(m_z[...], axis=0)
-    moment_out[...] = moment_own
-    gain = jnp.sum(wt_ref[...].astype(F32) * moment_own, axis=1, keepdims=True)
-    g_mine[...] = jnp.broadcast_to(gain, g_mine.shape)
-
-    def gy_copy(step):
-        return rdma(g_mine, g_y.at[y], gy_send.at[step], gy_recv.at[step],
-                    (z, x, c, lax.rem(y + step, NY)))
-
-    def gy_arrival(step):
-        source = lax.rem(y + NY - step, NY)
-        return rdma(g_mine, g_y.at[source], gy_send.at[step], gy_recv.at[step], (z, x, c, source))
-
-    for step in range(1, NY):
-        gy_copy(step).start()
-    g_y[y] = g_mine[...]
-
     for step in range(1, NY):
         ay_arrival(step).wait_recv()
         ay_copy(step).wait_send()
     aux_sum[...] = aux_y[0] + aux_y[1] + aux_y[2] + aux_y[3]
+    for k in range(HK):
+        az_out[k] = aux_sum[k : k + 1]
 
     def r_z_copy(k):
         target = lax.rem(z + 2 * NZ - 2 * k - c, NZ)
@@ -452,11 +493,11 @@
 
     def r_za_copy(k):
         target = lax.rem(z + 2 * NZ - 2 * k - c, NZ)
-        return rdma(aux_sum.at[k], aux_z.at[k], rza_send.at[k], rza_recv.at[k], (target, x, c, y))
+        return rdma(az_out.at[k], aux_z.at[k], rza_send.at[k], rza_recv.at[k], (target, x, c, y))
 
     r_z_home = [
         pltpu.make_async_copy(back.at[0], back_in.at[0], local_sem.at[4]),
-        pltpu.make_async_copy(aux_sum.at[0], aux_z.at[0], local_sem.at[5]),
+        pltpu.make_async_copy(az_out.at[0], aux_z.at[0], local_sem.at[5]),
     ]
 
     def send_back(k):
@@ -480,9 +521,48 @@
         back[pl.ds(h * half, half)] = (
             first[h, 0].astype(F32) + first_in[h, 0].astype(F32) + second_in[h].astype(F32)
         ).astype(BF)
-    for k in reversed(Z_ORDER):
+    for k in Z_ORDER:
         send_back(k)
 
+    m_z[0] = m_xsum[z]
+
+    @pl.loop(1, NZ)
+    def _(step):
+        mz_copy(step).wait()
+
+    moment_own = jnp.sum(m_z[...], axis=0)
+    ep_index = (z * NX + x) * NC + c
+    here = (moment_own.shape[0], NY * width)
+    is_own = iota(here, 1) == ep_index * here[0] + iota(here, 0)
+    own_gate = jnp.sum(jnp.where(is_own, mix_ref[...], 0.0), axis=1, keepdims=True)
+    dense_out[...] = moment_own * (own_gate * (1.0 / (NZ * NX * NC)))
+    gain = jnp.sum(wt_ref[...].astype(F32) * moment_own, axis=1, keepdims=True)
+    g_mine[...] = jnp.broadcast_to(gain, g_mine.shape)
+
+    def gy_copy(step):
+        return rdma(g_mine, g_y.at[y], gy_send.at[step], gy_recv.at[step],
+                    (z, x, c, lax.rem(y + step, NY)))
+
+    def gy_arrival(step):
+        source = lax.rem(y + NY - step, NY)
+        return rdma(g_mine, g_y.at[source], gy_send.at[step], gy_recv.at[step], (z, x, c, source))
+
+    for step in range(1, NY):
+        gy_copy(step).start()
+    g_y[y] = g_mine[...]
+
+    puts = [
+        pltpu.make_async_copy(source, target, put_sem.at[i])
+        for i, (source, target) in enumerate(((gate_s, gate_out), (up_s, up_out), (down_s, down_out)))
+    ]
+
+    def over_rows(a, b):
+        return dot(a, b, ROWS_BY)
+
+    down_s[...] = (
+        over_rows(hid[0], rows_of(grads_ref, 0)) + over_rows(hid[1], rows_of(grads_ref, 1))
+    ).astype(BF)
+    puts[2].start()
     for step in range(1, NY):
         gy_arrival(step).wait_recv()
     g_own[...] = g_y[0] + g_y[1] + g_y[2] + g_y[3]
@@ -502,14 +582,16 @@
 
     gain_out[z, x, c] = g_own[...]
 
-    def over_rows(a, b):
-        return dot(a, b, ROWS_BY)
-
-    grows = (rows_ref[pl.ds((1 - c) * HK, HK)].reshape(HALF, NY * width), rows_ref[pl.ds(c * HK, HK)].reshape(HALF, NY * width))
-    ggrads = (grads_ref[pl.ds((1 - c) * HK, HK)].reshape(HALF, NY * width), grads_ref[pl.ds(c * HK, HK)].reshape(HALF, NY * width))
-    gate_out[...] = (over_rows(grows[0], dg[0]) + over_rows(grows[1], dg[1])).astype(BF)
-    up_out[...] = (over_rows(grows[0], du[0]) + over_rows(grows[1], du[1])).astype(BF)
-    down_out[...] = (over_rows(hid[0], ggrads[0]) + over_rows(hid[1], ggrads[1])).astype(BF)
+    gate_s[...] = (
+        over_rows(dg[0], rows_of(rows_ref, 0)) + over_rows(dg[1], rows_of(rows_ref, 1))
+    ).astype(BF)
+    puts[0].start()
+    up_s[...] = (
+        over_rows(du[0], rows_of(rows_ref, 0)) + over_rows(du[1], rows_of(rows_ref, 1))
+    ).astype(BF)
+    puts[1].start()
+    scaled = (mix_ref[...] * full_ref[...].astype(F32)).astype(BF)
+    dx_acc[...] = dot(scaled, dense_ref[...].reshape(NY * width, width), PLAIN)
 
     @pl.loop(1, NZ)
     def _(step):
@@ -547,8 +629,8 @@
             r_z_copy(k).wait()
             r_za_copy(k).wait()
     permuted(perm_ref, back_in, sorted_back)
-    for q in range(NQ):
-        aux_t[q] = aux_z[:, q, :]
+    for k in range(HK):
+        aux_t[k : k + 1] = aux_z[k]
 
     def r_x_copy(step):
         other = lax.rem(me_q + step, NQ)
@@ -557,7 +639,7 @@
 
     def r_xa_copy(step):
         other = lax.rem(me_q + step, NQ)
-        return rdma(aux_t.at[other], aux_out.at[me_q], rxa_send.at[step], rxa_recv.at[step],
+        return rdma(aux_t, aux_out.at[me_q], rxa_send.at[step], rxa_recv.at[step],
                     (z, lax.rem(other, NX), other // NX, y))
 
     def r_x_arrival(step):
@@ -565,14 +647,14 @@
         device = (z, lax.rem(source, NX), source // NX, y)
         return (
             rdma(sorted_back.at[source], out_ref.at[source], rx_send.at[step], rx_recv.at[step], device),
-            rdma(aux_t.at[source], aux_out.at[source], rxa_send.at[step], rxa_recv.at[step], device),
+            rdma(aux_t, aux_out.at[source], rxa_send.at[step], rxa_recv.at[step], device),
         )
 
     for step in range(1, NQ):
         r_x_copy(step).start()
         r_xa_copy(step).start()
     out_ref[me_q] = sorted_back[me_q]
-    aux_out[me_q] = aux_t[me_q]
+    aux_out[me_q] = aux_t[...]
 
     for step in range(1, NX):
         gx_arrival(step).wait_recv()
@@ -581,6 +663,25 @@
     for step in range(1, NQ):
         for arrival in r_x_arrival(step):
             arrival.wait_recv()
+    token_out[...] = (
+        dx_acc[...] + dot(sel_ref[...], out_ref[...].reshape(NQ * BLK, width), ROWS_BY)
+    ).astype(BF)
+    group_of = ones_where(over_5(iota((NQ * BLK, HK * NQ), 0)) == iota((NQ * BLK, HK * NQ), 1), BF)
+    values = exact_dot(group_of, aux_out[...].reshape(HK * NQ, 128))
+    at = (NQ * BLK, 128)
+    lane_is = iota(at, 0) - CAP * over_5(iota(at, 0)) + me_q * CAP == iota(at, 1)
+    value = jnp.sum(jnp.where(lane_is, values, 0.0), axis=1, keepdims=True)
+    home_weights = weights_ref[...].astype(F32)
+    for p in range(2):
+        total = jnp.sum(chosen_ref[p] * value, axis=0, keepdims=True)
+        route_out[p : p + 1, :] = total / home_weights[p : p + 1, :]
+    tiles_in = gain_out[...].reshape(NZ * NX * NC * here[0], 128)
+    diagonal = ones_where(iota((128, 128), 0) == iota((128, 128), 1), F32)
+    for n in range(NZ * NX * NC * here[0] // 128):
+        picked = jnp.sum(tiles_in[n * 128 : (n + 1) * 128] * diagonal, axis=0, keepdims=True)
+        mix_out[n : n + 1, :] = picked * (1.0 / (NZ * NX * NC))
+    for copy in puts:
+        copy.wait()
     for step in range(1, NQ):
         r_x_copy(step).wait_send()
         r_xa_copy(step).wait_send()
@@ -631,27 +732,26 @@
 DMA = pltpu.SemaphoreType.DMA
 
 
-def layer(select, select_weighted, tokens, cotangent, wt, perm, pick, lane, gate, up, down):
+def layer(tokens, cotangent, routes, weights, wt, mix_gate, gate, up, down):
     width = tokens.shape[1]
     half = HK // 2
     own = wt.shape[0]
+    hidden = gate.shape[0]
     vm = pltpu.VMEM
     shape = jax.ShapeDtypeStruct
     return pl.pallas_call(
         layer_kernel,
         out_shape=(
-            shape((NQ, BLK, width), BF),
-            shape((NQ, HK, 128), F32),
-            shape((own, width), F32),
-            shape((NZ, NX, NC, own, 128), F32),
-            shape((tokens.shape[0], NY * width), BF),
-            shape((NZ, NX, NC) + wt.shape, BF),
+            shape(tokens.shape, BF),
+            shape(routes.shape, F32),
             shape(gate.shape, BF),
             shape(up.shape, BF),
             shape(down.shape, BF),
+            shape(wt.shape, F32),
+            shape((NY * width // 128, 128), F32),
         ),
-        in_specs=[VMEM_SPEC] * 8 + [HBM_SPEC] * 3,
-        out_specs=(VMEM_SPEC,) * 9,
+        in_specs=[VMEM_SPEC] * 6 + [HBM_SPEC] * 3,
+        out_specs=(VMEM_SPEC,) * 2 + (HBM_SPEC,) * 3 + (VMEM_SPEC,) * 2,
         scratch_shapes=[
             vm((NQ, BLK, width), BF),
             vm((NQ, BLK, width), BF),
@@ -664,23 +764,23 @@
             vm(gate.shape, BF),
             vm(gate.shape, BF),
             vm(down.shape, BF),
-            vm((2, HALF, gate.shape[1]), BF),
-            vm((2, HALF, gate.shape[1]), BF),
-            vm((2, HALF, gate.shape[1]), BF),
+            vm((2, HALF, hidden), BF),
+            vm((2, HALF, hidden), BF),
+            vm((2, HALF, hidden), BF),
             vm((2, HK, BLK, NY * width), BF),
             vm((HK, BLK, NY * width), BF),
-            vm((2, HK, NQ, 128), F32),
-            vm((HK, NQ, 128), F32),
+            vm((2, HK, 128), F32),
+            vm((HK, 128), F32),
             vm((2, NY, half, BLK, width), BF),
             vm((2, 2, half, BLK, width), BF),
             vm((2, half, BLK, width), BF),
             vm((HK, BLK, width), BF),
             vm((HK, BLK, width), BF),
             vm((NQ, BLK, width), BF),
-            vm((HK, NQ, 128), F32),
-            vm((NY, HK, NQ, 128), F32),
-            vm((HK, NQ, 128), F32),
-            vm((NQ, HK, 128), F32),
+            vm((HK, 128), F32),
+            vm((NY, HK, 128), F32),
+            vm((HK, 1, 128), F32),
+            vm((HK, 128), F32),
             vm((NZ, NX, NC, own, width), F32),
             vm((NZ, NX, own, width), F32),
             vm((NZ, NX, own, width), F32),
@@ -741,59 +841,64 @@
             DMA((NX,)),
             DMA((1,)),
             DMA((1,)),
+            vm((NQ * BLK, NQ * BLK), BF),
+            vm((NQ * BLK, tokens.shape[0]), BF),
+            vm((2, NQ * BLK, tokens.shape[0]), F32),
+            vm((tokens.shape[0], NY * width), BF),
+            vm((NZ, NX, NC) + wt.shape, BF),
+            vm((NQ, BLK, width), BF),
+            vm((NQ, HK, 128), F32),
+            vm((HK, 1, 128), F32),
+            vm((NZ, NX, NC, own, 128), F32),
+            vm((2, HALF, hidden), F32),
+            vm((2, HALF, hidden), F32),
+            vm(tokens.shape, F32),
+            vm(gate.shape, BF),
+            vm(gate.shape, BF),
+            vm(down.shape, BF),
+            DMA((3,)),
         ],
         compiler_params=pltpu.CompilerParams(
             collective_id=0, has_side_effects=True, vmem_limit_bytes=60 * 1024 * 1024
         ),
         name="layer",
-    )(select, select_weighted, tokens, cotangent, wt, perm, pick, lane, gate, up, down)
+    )(tokens, cotangent, routes, weights, wt, mix_gate, gate, up, down)
+
+
+def put_kernel(count, *refs):
+    ins, outs, held, sems = refs[:count], refs[count : 2 * count], refs[2 * count : -1], refs[-1]
+    first = [pltpu.make_async_copy(ins[i], held[i], sems.at[0, i]) for i in range(count)]
+    second = [pltpu.make_async_copy(held[i], outs[i], sems.at[1, i]) for i in range(count)]
+    for copy in first:
+        copy.start()
+    for i in range(count):
+        first[i].wait()
+        second[i].start()
+    for copy in second:
+        copy.wait()
+
+
+def put_out(values):
+    return pl.pallas_call(
+        functools.partial(put_kernel, len(values)),
+        out_shape=tuple(jax.ShapeDtypeStruct(v.shape, v.dtype) for v in values),
+        in_specs=[HBM_SPEC] * len(values),
+        out_specs=(HBM_SPEC,) * len(values),
+        scratch_shapes=[pltpu.VMEM(v.shape, v.dtype) for v in values] + [DMA((2, len(values)))],
+        compiler_params=pltpu.CompilerParams(vmem_limit_bytes=60 * 1024 * 1024),
+        name="put_out",
+    )(*values)
 
 
 def local(tokens, cotangent, routes, route_weights, w_gate, w_up, w_down, dense_weight, mix_gate):
-    z, x, c = (lax.axis_index(a) for a in EP)
-    token_count = routes.shape[0]
-    ep_count = NZ * NX * NC
-    e = jnp.arange(EXPERTS, dtype=jnp.int32)
-    expert = lax.rem(z + 2 * lax.rem(e, HK) + e // (HK * NX), NZ) * NX + lax.rem(e // HK, NX)
-    picked = routes.T
-    hits = [picked[p][None, :] == expert[:, None] for p in range(2)]
-    hit = hits[0] | hits[1]
-    t = jnp.arange(token_count, dtype=jnp.int32)
-    earlier = (t[:, None] < t[None, :]).astype(BF)
-    rank = jnp.dot(hit.astype(BF), earlier, preferred_element_type=F32).astype(jnp.int32)
-    s = jnp.arange(CAP, dtype=jnp.int32)
-    chosen = (hit[:, None, :] & (rank[:, None, :] == s[None, :, None])).reshape(-1, token_count)
-    weights = route_weights.T
-    weight = jnp.where(hits[0], weights[0][None, :], weights[1][None, :])
-    weight = jnp.broadcast_to(weight[:, None, :], (EXPERTS, CAP, token_count)).reshape(-1, token_count)
-    select = chosen.astype(BF)
-    select_weighted = jnp.where(chosen, weight, jnp.zeros_like(weight))
-    r = jnp.arange(NQ * BLK, dtype=jnp.int32)
-    moved = lax.rem(r, BLK) // CAP * BLK + r // BLK * CAP + lax.rem(r, CAP)
-    perm = (moved[:, None] == r[None, :]).astype(BF)
-    groups = jnp.arange(HK * NQ, dtype=jnp.int32)
-    pick = (r[None, :] // CAP == groups[:, None]).astype(BF)
-    lane = (lax.rem(r, CAP)[:, None] == jnp.arange(128, dtype=jnp.int32)[None, :]).astype(F32)
-    slots, aux_back, moment_own, gain_all, cot_full, wt_full, gate_grad, up_grad, down_grad = layer(
-        select, select_weighted, tokens, cotangent, dense_weight.T, perm, pick, lane,
-        w_gate[0], w_up[0], w_down[0],
+    token_grad, route_grad, gate_grad, up_grad, down_grad, dense_grad, mix_grad = put_out(layer(
+        tokens, cotangent, routes.T, route_weights.T, dense_weight.T, mix_gate.reshape(1, -1),
+        w_gate[0].T, w_up[0].T, w_down[0],
+    ))
+    return (
+        token_grad, route_grad.T, gate_grad.T[None], up_grad.T[None], down_grad[None],
+        dense_grad.T, mix_grad.reshape(-1),
     )
-    own = dense_weight.shape[1]
-    wt_full = wt_full.reshape(ep_count * own, -1)
-    scaled = (mix_gate[None, :] * cot_full.astype(F32)).astype(BF)
-    dense_dx = jnp.dot(scaled, wt_full, preferred_element_type=F32)
-    token_grad = (dense_dx + dot(select, slots.reshape(NQ * BLK, -1), ROWS_BY)).astype(BF)
-    values = aux_back[:, :, :CAP].reshape(EXPERTS, CAP)
-    at_slot = jnp.sum(
-        jnp.where(rank[:, :, None] == s[None, None, :], values[:, None, :], 0.0), axis=2
-    )
-    route_sums = jnp.stack([jnp.sum(jnp.where(h, at_slot, 0.0), axis=0) for h in hits], axis=1)
-    route_grad = route_sums / route_weights.astype(F32)
-    ep_index = (z * NX + x) * NC + c
-    own_gate = lax.dynamic_slice(mix_gate, (ep_index * own,), (own,))
-    dense_grad = (moment_own * (own_gate[:, None] * (1.0 / ep_count))).T
-    mix_grad = gain_all[..., 0].reshape(-1) / ep_count
-    return token_grad, route_grad, gate_grad[None], up_grad[None], down_grad[None], dense_grad, mix_grad
 
 
 def solution(mesh):

time: 115 us -> 95.1 us (0.83)
  local copies, waits for them, and re-layouts: 8.59 us -> 0 us
  other arithmetic: 5.68 us -> 0 us
  matrix products: 3.25 us -> 0 us
  Pallas kernels: 96 us -> 94.2 us
    unnamed x27 -> x0, local copies, waits for them, and re-layouts: 6.58 us -> none
    dot_general x3 -> x0, matrix products: 3.25 us -> none  [the longest x1 1.82 us: local(): dense_dx = jnp.dot(scaled, wt_full, preferred_element_type=F32)]
    convert_element_type x4 -> x0, other arithmetic: 2.87 us -> none  [the longest x1 0.81 us: local(): perm = (moved[:, None] == r[None, :]).astype(BF)]
    pallas_call x1 -> x2, Pallas kernels: 96 us -> 94.2 us  [the longest x1 91.6 us: layer(): pl.pallas_call(layer_kernel, out_shape=(shape(tokens.shape, BF), shape(ro...]
where the time goes in v3:
time: 95.1 us; the launch traced here: 94.9 us
  Pallas kernels  94.2 us (99%)
    pallas_call x1, Pallas kernels, layer(): pl.pallas_call(layer_kernel, out_shape=(shape(tokens.shape, BF), shape(ro...  91.6 us
    pallas_call x1, Pallas kernels, put_out(): pl.pallas_call(functools.partial(put_kernel, len(values)), out_shape=tupl...  2.61 us

profile of v3, /device:TPU:1, one launch (start us, length us, event | category | flops | bytes accessed | tf_op | source)
XLA Modules:
  0.0 94.9 jit_solution(14046938711659127949)
XLA Ops:
  0.6 91.6 %layer.1 = (bf16[128,256]{1,0:T(8,128)(2,1)}, f32[2,128]{1,0:T(2,128)}, bf16[352,1024]{1,0:T(8,128)(2,1)}, bf16[352,1024]{1,0:T(8,128)(2,1)}, bf16[352,1024]{1,0...) custom-call(bf16[128,256]{1,0:T(8,128)(2,1)} %tokens_ref.1, bf16[128,256]{1,0:T(8,128)(2,1)} %cot_ref.1, ...), custom_call_target="tpu_custom_call" | custom-call | tf_op jit(solution)/shard_map/layer/pallas_call | solution.py:742
  92.3 2.6 %put_out.1 = (bf16[128,256]{1,0:T(8,128)(2,1)}, f32[2,128]{1,0:T(2,128)}, bf16[352,1024]{1,0:T(8,128)(2,1)}, bf16[352,1024]{1,0:T(8,128)(2,1)}, bf16[352,1024]{1...) custom-call(bf16[128,256]{1,0:T(8,128)(2,1)} %get-tuple-element.21.refs_0_, f32[2,128]{1,0:T(2,128)} %get-tuple-element.22.refs_1_, ...), custom_call_target="tpu_custom_call" | custom-call | tf_op jit(solution)/shard_map/put_out/pallas_call | solution.py:882

commit v4 on v3

--- a/solution.py
+++ b/solution.py
@@ -65,8 +65,8 @@
 
 
 HALF = HK * BLK
-LAG_F = 3
-LAG_C = 6
+LAG_F = 6
+LAG_C = 12
 PLAIN = (((1,), (0,)), ((), ()))
 ROWS_BY = (((0,), (0,)), ((), ()))
 COLS_BY = (((1,), (1,)), ((), ()))
@@ -104,7 +104,7 @@
 
 
 def layer_kernel(
-    tokens_ref, cot_ref, routes_ref, weights_ref, wt_ref, mix_ref,
+    tokens_hbm, cot_hbm, routes_hbm, weights_hbm, wt_hbm, mix_hbm,
     wg_hbm, wu_hbm, wd_hbm,
     token_out, route_out, gate_out, up_out, down_out, dense_out, mix_out,
     *scratch,
@@ -121,6 +121,7 @@
         gc_recv,
         perm_ref, sel_ref, chosen_ref, full_ref, dense_ref, out_ref, aux_out, az_out, gain_out, pg, pu, dx_acc,
         gate_s, up_s, down_s, put_sem,
+        tokens_ref, cot_ref, routes_ref, weights_ref, wt_ref, mix_ref, in_sem,
     ) = scratch
     z, x, c, y = where_am_i()
     width = tokens_ref.shape[-1]
@@ -137,7 +138,14 @@
         pltpu.make_async_copy(cot_ref, full_ref.at[:, cols(y, width)], local_sem.at[0]),
         pltpu.make_async_copy(wt_ref, dense_ref.at[z, x, c], local_sem.at[1]),
     ]
-    for copy in own:
+    inputs = [
+        pltpu.make_async_copy(source, target, in_sem.at[i])
+        for i, (source, target) in enumerate((
+            (routes_hbm, routes_ref), (weights_hbm, weights_ref), (tokens_hbm, tokens_ref),
+            (cot_hbm, cot_ref), (wt_hbm, wt_ref), (mix_hbm, mix_ref),
+        ))
+    ]
+    for copy in inputs:
         copy.start()
     weights = [
         pltpu.make_async_copy(wg_hbm, wg, local_sem.at[6]),
@@ -147,6 +155,10 @@
     for copy in weights:
         copy.start()
     greet_all()
+    for copy in inputs:
+        copy.wait()
+    for copy in own:
+        copy.start()
     table = (NQ * BLK, tokens_ref.shape[0])
     row = iota(table, 0)
     line = over_40(row)
@@ -169,6 +181,58 @@
     select_weighted = (chosen_ref[0] * gate_weights[0:1, :] + chosen_ref[1] * gate_weights[1:2, :]).astype(BF)
     slots[0][...] = gathered_rows(select, tokens_ref)
     slots[1][...] = gathered_rows(select_weighted, cot_ref)
+    wait_all()
+
+    def x_copy(a, step):
+        other = lax.rem(me_q + step, NQ)
+        return rdma(
+            slots[a].at[other], gathered[a].at[me_q], x_send.at[a, step], x_recv.at[a, step],
+            (z, lax.rem(other, NX), other // NX, y),
+        )
+
+    def x_arrival(a, step):
+        source = lax.rem(me_q + NQ - step, NQ)
+        return rdma(
+            slots[a].at[source], gathered[a].at[source], x_send.at[a, step], x_recv.at[a, step],
+            (z, lax.rem(source, NX), source // NX, y),
+        )
+
+    for a in range(2):
+        for step in range(1, NQ):
+            x_copy(a, step).start()
+
+    def g_copy(step):
+        return rdma(
+            cot_ref, full_ref.at[:, cols(y, width)], g_send.at[step], g_recv.at[step],
+            (z, x, c, lax.rem(y + step, NY)),
+        )
+
+    def g_arrival(step):
+        source = lax.rem(y + NY - step, NY)
+        return rdma(
+            cot_ref, full_ref.at[:, cols(source, width)], g_send.at[step], g_recv.at[step],
+            (z, x, c, source),
+        )
+
+    for step in range(1, NY):
+        g_copy(step).start()
+
+    def dz_copy(step):
+        return rdma(
+            wt_ref, dense_ref.at[z, x, c], dz_send.at[step], dz_recv.at[step],
+            (lax.rem(z + step, NZ), x, c, y),
+        )
+
+    def dz_arrival(step):
+        source = lax.rem(z + NZ - step, NZ)
+        return rdma(
+            wt_ref, dense_ref.at[source, x, c], dz_send.at[step], dz_recv.at[step], (source, x, c, y)
+        )
+
+    @pl.loop(1, NZ)
+    def _(step):
+        dz_copy(step).start()
+
     both_ways = (NQ * BLK, NQ * BLK)
     place = iota(both_ways, 0)
     block = over_40(place)
@@ -177,57 +241,6 @@
     perm_ref[...] = ones_where(
         source * BLK + block * CAP + (inside - CAP * source) == iota(both_ways, 1), BF
     )
-    wait_all()
-
-    def x_copy(a, step):
-        other = lax.rem(me_q + step, NQ)
-        return rdma(
-            slots[a].at[other], gathered[a].at[me_q], x_send.at[a, step], x_recv.at[a, step],
-            (z, lax.rem(other, NX), other // NX, y),
-        )
-
-    def x_arrival(a, step):
-        source = lax.rem(me_q + NQ - step, NQ)
-        return rdma(
-            slots[a].at[source], gathered[a].at[source], x_send.at[a, step], x_recv.at[a, step],
-            (z, lax.rem(source, NX), source // NX, y),
-        )
-
-    for a in range(2):
-        for step in range(1, NQ):
-            x_copy(a, step).start()
-
-    def g_copy(step):
-        return rdma(
-            cot_ref, full_ref.at[:, cols(y, width)], g_send.at[step], g_recv.at[step],
-            (z, x, c, lax.rem(y + step, NY)),
-        )
-
-    def g_arrival(step):
-        source = lax.rem(y + NY - step, NY)
-        return rdma(
-            cot_ref, full_ref.at[:, cols(source, width)], g_send.at[step], g_recv.at[step],
-            (z, x, c, source),
-        )
-
-    for step in range(1, NY):
-        g_copy(step).start()
-
-    def dz_copy(step):
-        return rdma(
-            wt_ref, dense_ref.at[z, x, c], dz_send.at[step], dz_recv.at[step],
-            (lax.rem(z + step, NZ), x, c, y),
-        )
-
-    def dz_arrival(step):
-        source = lax.rem(z + NZ - step, NZ)
-        return rdma(
-            wt_ref, dense_ref.at[source, x, c], dz_send.at[step], dz_recv.at[step], (source, x, c, y)
-        )
-
-    @pl.loop(1, NZ)
-    def _(step):
-        dz_copy(step).start()
 
     def z_copy(a, k):
         target = lax.rem(z + 2 * k + c, NZ)
@@ -368,13 +381,13 @@
                 m_half[:, n] = moment_ref[:, n, c] + m_in[:, n]
             for step in range(1, NX):
                 mx_copy(step).start()
-        if i == 13:
+        if i == 19:
             for copy in weights:
                 copy.wait()
             for k in Z_ORDER:
                 c_arrival(0, k).wait_recv()
-        if 14 <= i < 18:
-            turn = (i - 14) // 2
+        if 20 <= i < 24:
+            turn = (i - 20) // 2
             if i % 2 == 0:
                 pg[turn] = dot(rows_of(rows_ref, turn), wg[...], COLS_BY)
             else:
@@ -382,7 +395,7 @@
         if i == 20:
             for step in range(1, NX):
                 mx_copy(step).wait_recv()
-            m_xsum[...] = m_half[:, x] + m_x[0] + m_x[1] + m_x[2]
+            m_xsum[...] = (m_half[:, x] + m_x[0] + m_x[1] + m_x[2]).astype(BF)
 
             @pl.loop(1, NZ)
             def _(step):
@@ -521,7 +534,7 @@
         back[pl.ds(h * half, half)] = (
             first[h, 0].astype(F32) + first_in[h, 0].astype(F32) + second_in[h].astype(F32)
         ).astype(BF)
-    for k in Z_ORDER:
+    for k in reversed(Z_ORDER):
         send_back(k)
 
     m_z[0] = m_xsum[z]
@@ -530,7 +543,7 @@
     def _(step):
         mz_copy(step).wait()
 
-    moment_own = jnp.sum(m_z[...], axis=0)
+    moment_own = jnp.sum(m_z[...].astype(F32), axis=0)
     ep_index = (z * NX + x) * NC + c
     here = (moment_own.shape[0], NY * width)
     is_own = iota(here, 1) == ep_index * here[0] + iota(here, 0)
@@ -750,7 +763,7 @@
             shape(wt.shape, F32),
             shape((NY * width // 128, 128), F32),
         ),
-        in_specs=[VMEM_SPEC] * 6 + [HBM_SPEC] * 3,
+        in_specs=[HBM_SPEC] * 9,
         out_specs=(VMEM_SPEC,) * 2 + (HBM_SPEC,) * 3 + (VMEM_SPEC,) * 2,
         scratch_shapes=[
             vm((NQ, BLK, width), BF),
@@ -785,8 +798,8 @@
             vm((NZ, NX, own, width), F32),
             vm((NZ, NX, own, width), F32),
             vm((NX - 1, NZ, own, width), F32),
-            vm((NZ, own, width), F32),
-            vm((NZ, own, width), F32),
+            vm((NZ, own, width), BF),
+            vm((NZ, own, width), BF),
             vm((own, 128), F32),
             vm((own, 128), F32),
             vm((NY, own, 128), F32),
@@ -857,6 +870,13 @@
             vm(gate.shape, BF),
             vm(down.shape, BF),
             DMA((3,)),
+            vm(tokens.shape, BF),
+            vm(tokens.shape, BF),
+            vm(routes.shape, jnp.int32),
+            vm(weights.shape, BF),
+            vm(wt.shape, BF),
+            vm(mix_gate.shape, F32),
+            DMA((6,)),
         ],
         compiler_params=pltpu.CompilerParams(
             collective_id=0, has_side_effects=True, vmem_limit_bytes=60 * 1024 * 1024

time: 95.1 us -> 90.9 us (0.956)
  Pallas kernels: 94.2 us -> 89.8 us
    pallas_call x1, Pallas kernels: 91.6 us -> 87.2 us  [layer(): pl.pallas_call(layer_kernel, out_shape=(shape(tokens.shape, BF), shape(ro...]
where the time goes in v4:
time: 90.9 us; the launch traced here: 90.4 us
  Pallas kernels  89.8 us (99%)
    pallas_call x1, Pallas kernels, layer(): pl.pallas_call(layer_kernel, out_shape=(shape(tokens.shape, BF), shape(ro...  87.2 us
    pallas_call x1, Pallas kernels, put_out(): pl.pallas_call(functools.partial(put_kernel, len(values)), out_shape=tupl...  2.61 us

profile of v4, /device:TPU:1, one launch (start us, length us, event | category | flops | bytes accessed | tf_op | source)
XLA Modules:
  0.0 90.4 jit_solution(13463624724807830566)
XLA Ops:
  0.6 87.2 %layer.1 = (bf16[128,256]{1,0:T(8,128)(2,1)}, f32[2,128]{1,0:T(2,128)}, bf16[352,1024]{1,0:T(8,128)(2,1)}, bf16[352,1024]{1,0:T(8,128)(2,1)}, bf16[352,1024]{1,0...) custom-call(bf16[128,256]{1,0:T(8,128)(2,1)} %tokens_hbm.1, bf16[128,256]{1,0:T(8,128)(2,1)} %cot_hbm.1, ...), custom_call_target="tpu_custom_call" | custom-call | tf_op jit(solution)/shard_map/layer/pallas_call | solution.py:755
  87.8 2.6 %put_out.1 = (bf16[128,256]{1,0:T(8,128)(2,1)}, f32[2,128]{1,0:T(2,128)}, bf16[352,1024]{1,0:T(8,128)(2,1)}, bf16[352,1024]{1,0:T(8,128)(2,1)}, bf16[352,1024]{1...) custom-call(bf16[128,256]{1,0:T(8,128)(2,1)} %get-tuple-element.21.refs_0_, f32[2,128]{1,0:T(2,128)} %get-tuple-element.22.refs_1_, ...), custom_call_target="tpu_custom_call" | custom-call | tf_op jit(solution)/shard_map/put_out/pallas_call | solution.py:902
